TPU v7x, 32 devices: a whole 2x2x4 slice. The times are simulated.
32 devices in a mesh: sp: 8 (over z, x), dp: 4 (over y, core).
Axes of the slice: x: 2, y: 2, z: 4, core: 2. Of those that a mesh axis runs over, the one named last changes fastest.
Arguments:
- lin_pre: bfloat16 [2048, 8192], P(None, ('dp', 'sp')), may hold values from -6 to 6
- gate_pre: bfloat16 [2048, 8192], P(None, ('dp', 'sp')), may hold values from -8 to 8
- w_depth: float32 [31, 2048], replicated, may hold values from -1 to 1
- ln_gain: float32 [2048], replicated, may hold values from 0.1 to 1.9
- ln_shift: float32 [2048], replicated, may hold values from -3 to 3
- w_out: bfloat16 [2048, 2048], P(None, 'dp'), may hold values from -0.125 to 0.125
Outputs:
- module_out: bfloat16 [8192, 2048], P(('dp', 'sp'))
All inputs are finite; a program needn't handle non-finite values.
Results may differ from a plain program's by a relative error of at most 0.0064.
Values may be sent and summed in bfloat16 or wider, within the bound.
No kernel may reach another device: no remote copies, remote signals or barrier semaphores. Data moves between devices by JAX's collectives and lax.ppermute only.
A program may use at most 64 MiB of HBM per device.

v0:
```python
import functools

import jax
import jax.numpy as jnp
from jax import lax
from jax.experimental import pallas as pl
from jax.experimental.pallas import tpu as pltpu
from jax.sharding import PartitionSpec as P


LANES = 128
EDGE = 16
EPS = 1e-05


def params(semantics=None):
    return pltpu.CompilerParams(dimension_semantics=semantics, vmem_limit_bytes=16 << 20)


def cost(flops, nbytes):
    return pl.CostEstimate(flops=flops, transcendentals=0, bytes_accessed=nbytes)


def glu_body(lin_ref, gate_ref, out_ref, head_ref, tail_ref):
    gate = gate_ref[...].astype(jnp.float32)
    glu = (lin_ref[...].astype(jnp.float32) * jax.nn.sigmoid(gate)).T.astype(jnp.bfloat16)
    out_ref[...] = glu
    head_ref[...] = glu[:EDGE]
    tail_ref[...] = glu[glu.shape[0] - EDGE :]


def gated(lin_pre, gate_pre):
    channels, tokens = lin_pre.shape
    block = 256
    edge = pl.BlockSpec((EDGE, block), lambda i: (0, i))
    return pl.pallas_call(
        glu_body,
        grid=(channels // block,),
        in_specs=[pl.BlockSpec((block, tokens), lambda i: (i, 0))] * 2,
        out_specs=[pl.BlockSpec((tokens, block), lambda i: (0, i)), edge, edge],
        out_shape=[
            jax.ShapeDtypeStruct((tokens, channels), jnp.bfloat16),
            jax.ShapeDtypeStruct((EDGE, channels), jnp.bfloat16),
            jax.ShapeDtypeStruct((EDGE, channels), jnp.bfloat16),
        ],
        compiler_params=params(("arbitrary",)),
        cost_estimate=cost(20 * channels * tokens, 6 * channels * tokens),
        name="glu",
    )(lin_pre, gate_pre)


def conv_norm(cells, w_ref, gain_ref, shift_ref, mixed, start, tiles, store):
    blocks = cells.shape[0]
    span = 8 * tiles
    channels = blocks * LANES
    taps = w_ref.shape[0]

    def one_block(block, total):
        lanes = pl.ds(pl.multiple_of(block * LANES, LANES), LANES)
        running = [jnp.zeros((span, LANES), jnp.float32) for _ in range(2)]
        turn = 0
        lead = EDGE - (taps - 1) // 2
        for phase in range(8):
            window = cells[block, pl.ds(start - EDGE + phase, span + 8 * 3), :]
            for whole in range(4):
                tap = 8 * whole + phase - lead
                if 0 <= tap < taps:
                    weight = w_ref[pl.ds(tap, 1), lanes]
                    running[turn] = running[turn] + weight * window[8 * whole : 8 * whole + span]
                    turn = 1 - turn
        value = (running[0] + running[1]).astype(jnp.bfloat16).astype(jnp.float32)
        mixed[block, pl.ds(0, span), :] = value
        return total + value

    zeros = jnp.zeros((span, LANES), jnp.float32)
    total = lax.fori_loop(0, blocks, one_block, zeros)
    mean = jnp.broadcast_to(jnp.sum(total, axis=1, keepdims=True) / channels, (span, LANES))

    square = zeros
    for block in range(blocks):
        square = square + jnp.square(mixed[block, pl.ds(0, span), :] - mean)
    variance = jnp.sum(square, axis=1, keepdims=True) / channels
    scale = jnp.broadcast_to(lax.rsqrt(variance + EPS), (span, LANES))
    for block in range(blocks):
        lanes = pl.ds(block * LANES, LANES)
        normed = (mixed[block, pl.ds(0, span), :] - mean) * scale
        normed = normed * gain_ref[:, lanes] + shift_ref[:, lanes]
        store(lanes, (normed * jax.nn.sigmoid(normed)).astype(jnp.bfloat16))


def inner_body(tiles, glu_ref, w_ref, gain_ref, shift_ref, out_ref, cells, mixed):
    blocks = cells.shape[0]
    for block in range(blocks):
        cells[block] = glu_ref[:, pl.ds(block * LANES, LANES)].astype(jnp.float32)
    span = 8 * tiles

    def chunk(i, carry):
        start = pl.multiple_of(EDGE + i * span, 8)

        def store(lanes, value):
            out_ref[pl.ds(start, span), lanes] = value

        conv_norm(cells, w_ref, gain_ref, shift_ref, mixed, start, tiles, store)
        return carry

    lax.fori_loop(0, (glu_ref.shape[0] - 2 * EDGE) // span, chunk, 0)


def outer_body(before_ref, after_ref, glu_ref, w_ref, gain_ref, shift_ref, _, out_ref, cells, mixed):
    side = pl.program_id(0)
    blocks = cells.shape[0]
    for block in range(blocks):
        lanes = pl.ds(block * LANES, LANES)
        own = glu_ref[:, lanes].astype(jnp.float32)
        halo = jnp.where(side == 0, before_ref[:, lanes], after_ref[:, lanes]).astype(jnp.float32)
        cells[block, pl.ds(EDGE, 2 * EDGE), :] = jnp.where(side == 0, own, 0.0)
        cells[block, pl.ds(0, EDGE), :] = jnp.where(side == 0, halo, own[:EDGE])
        cells[block, pl.ds(EDGE, EDGE), :] = jnp.where(side == 0, own[:EDGE], own[EDGE:])
        cells[block, pl.ds(2 * EDGE, EDGE), :] = jnp.where(side == 0, own[EDGE:], halo)

    def store(lanes, value):
        out_ref[:, lanes] = value

    conv_norm(cells, w_ref, gain_ref, shift_ref, mixed, EDGE, EDGE // 8, store)


def activated_inner(glu, w_depth, gain, shift):
    tokens, channels = glu.shape
    inner = (tokens - 2 * EDGE) // 16
    tiles = 2 * max(n for n in range(1, 5) if inner % n == 0)
    blocks = channels // LANES
    return pl.pallas_call(
        functools.partial(inner_body, tiles),
        out_shape=jax.ShapeDtypeStruct((tokens, channels), jnp.bfloat16),
        scratch_shapes=[
            pltpu.VMEM((blocks, tokens, LANES), jnp.float32),
            pltpu.VMEM((blocks, 8 * tiles, LANES), jnp.float32),
        ],
        compiler_params=params(),
        cost_estimate=cost(80 * channels * tokens, 4 * channels * tokens),
        name="conv_inner",
    )(glu, w_depth, gain, shift)


def activated_outer(before, after, glu, w_depth, gain, shift, act):
    tokens, channels = glu.shape
    blocks = channels // LANES
    whole = pl.BlockSpec((EDGE, channels), lambda i: (0, 0))
    row = pl.BlockSpec((1, channels), lambda i: (0, 0))
    last = tokens // EDGE - 1
    return pl.pallas_call(
        outer_body,
        grid=(2,),
        in_specs=[
            whole,
            whole,
            pl.BlockSpec((2 * EDGE, channels), lambda i: (i * (tokens // (2 * EDGE) - 1), 0)),
            pl.BlockSpec(w_depth.shape, lambda i: (0, 0)),
            row,
            row,
            pl.BlockSpec(memory_space=pl.ANY),
        ],
        out_specs=pl.BlockSpec((EDGE, channels), lambda i: (i * last, 0)),
        out_shape=jax.ShapeDtypeStruct((tokens, channels), jnp.bfloat16),
        scratch_shapes=[
            pltpu.VMEM((blocks, 3 * EDGE, LANES), jnp.float32),
            pltpu.VMEM((blocks, EDGE, LANES), jnp.float32),
        ],
        input_output_aliases={6: 0},
        compiler_params=params(("arbitrary",)),
        cost_estimate=cost(80 * channels * 2 * EDGE, 8 * channels * EDGE),
        name="conv_outer",
    )(before, after, glu, w_depth, gain, shift, act)


WHOLE = pl.BlockSpec(memory_space=pltpu.VMEM)
STAY = pl.BlockSpec(memory_space=pltpu.HBM)
TABLE = pl.BlockSpec(memory_space=pltpu.SMEM)


def quarters_body(place_ref, w_ref, *refs):
    outs, sems = refs[:-1], refs[-1]
    rows = outs[0].shape[0]
    copies = [
        pltpu.make_async_copy(w_ref.at[pl.ds(place_ref[i] * rows, rows), :], out, sems.at[i])
        for i, out in enumerate(outs)
    ]
    for copy in copies:
        copy.start()
    for copy in copies:
        copy.wait()


def quarters(w_out, units):
    shape = jax.ShapeDtypeStruct((w_out.shape[0] // 4, w_out.shape[1]), w_out.dtype)
    return pl.pallas_call(
        quarters_body,
        in_specs=[TABLE, STAY],
        out_specs=[WHOLE] * len(units),
        out_shape=[shape] * len(units),
        scratch_shapes=[pltpu.SemaphoreType.DMA((len(units),))],
        compiler_params=params(),
        name="quarters",
    )(jnp.stack(units), pltpu.with_memory_space_constraint(w_out, pltpu.HBM))


def project_body(place_ref, act_ref, *refs):
    chunks, out_ref = refs[:-1], refs[-1]
    rows = chunks[0].shape[0]
    total = None
    for i, chunk in enumerate(chunks):
        if len(chunks) == 1:
            part = act_ref[...]
        else:
            part = act_ref[:, pl.ds(pl.multiple_of(place_ref[i] * rows, LANES), rows)]
        term = jnp.dot(part, chunk[...], preferred_element_type=jnp.float32)
        total = term if total is None else total + term
    out_ref[...] = total.astype(jnp.bfloat16)


def project(act, chunks, units):
    tokens, channels = act.shape
    width = chunks[0].shape[1]
    return pl.pallas_call(
        project_body,
        in_specs=[TABLE] + [WHOLE] * (1 + len(chunks)),
        out_specs=WHOLE,
        out_shape=jax.ShapeDtypeStruct((tokens, width), jnp.bfloat16),
        compiler_params=params(),
        cost_estimate=cost(2 * tokens * channels * width, 2 * channels * (tokens + width)),
        name="project",
    )(jnp.stack(units), act, *chunks)


def collect_body(place_ref, *refs):
    pieces, out_ref, sems = refs[:-2], refs[-2], refs[-1]
    width = pieces[0].shape[1]
    copies = []
    for i, piece in enumerate(pieces):
        at = pl.multiple_of(place_ref[i] * width, LANES)
        copies.append(pltpu.make_async_copy(piece, out_ref.at[:, pl.ds(at, width)], sems.at[i]))
    for copy in copies:
        copy.start()
    for copy in copies:
        copy.wait()


def collect(pieces, shards):
    tokens, width = pieces[0].shape
    return pl.pallas_call(
        collect_body,
        in_specs=[TABLE] + [WHOLE] * len(pieces),
        out_specs=STAY,
        out_shape=jax.ShapeDtypeStruct((tokens, width * len(pieces)), jnp.bfloat16),
        scratch_shapes=[pltpu.SemaphoreType.DMA((len(pieces),))],
        compiler_params=params(),
        name="collect",
    )(jnp.stack(shards), *pieces)


def per_device(lin_pre, gate_pre, w_depth, ln_gain, ln_shift, w_out):
    dp, sp = lax.axis_size("dp"), lax.axis_size("sp")
    chips = dp // 2
    mine = lax.axis_index("dp")
    spot = lax.axis_index("sp") % 4

    def to_sibling(x):
        return lax.ppermute(x, "dp", [(i, i ^ 1) for i in range(dp)])

    def to_near(x, bit):
        return lax.ppermute(x, "sp", [(i, i ^ bit) for i in range(sp)])

    first, second = quarters(w_out, (spot, 3 - spot))
    hops = [
        [(i, (i // 2 + k) % chips * 2 + i % 2) for i in range(dp)] for k in range(1, chips)
    ]
    direct_a = [lax.ppermute(first, "dp", perm) for perm in hops]
    direct_b = [lax.ppermute(second, "dp", perm) for perm in hops]

    glu, head, tail = gated(lin_pre, gate_pre)
    ends = sp - 1
    before = lax.ppermute(tail, "sp", [(i, i + 1) for i in range(ends)])
    after = lax.ppermute(head, "sp", [(i + 1, i) for i in range(ends)])
    gain, shift = ln_gain[None, :], ln_shift[None, :]
    act = activated_inner(glu, w_depth, gain, shift)
    direct_a, act = lax.optimization_barrier((direct_a, act))
    by_x = [to_near(a, 1) for a in direct_a]
    by_z = [to_near(a, 2) for a in direct_a]
    before, after, act = lax.optimization_barrier((before, after, act))
    act = activated_outer(before, after, glu, w_depth, gain, shift, act)

    act_far = to_sibling(act)
    pieces, shards = [project(act, [w_out], (spot,))], [mine]
    own_far = project(act_far, [w_out], (spot,))
    received = [to_sibling(own_far)]
    by_x, by_z, direct_b, act_far, act, pieces = lax.optimization_barrier(
        (by_x, by_z, direct_b, act_far, act, pieces)
    )
    units = (spot, 3 - spot, spot ^ 1, spot ^ 2)
    for k in range(1, chips):
        near = [direct_a[k - 1], direct_b[k - 1], by_x[k - 1], by_z[k - 1]]
        other_far = project(act_far, near, units)
        received.append(to_sibling(other_far))
        pieces.append(project(act, near, units))
        shards.append((mine // 2 - k) % chips * 2 + mine % 2)
    return collect(pieces + received, shards + [shard ^ 1 for shard in shards])


def solution(mesh):
    in_specs = (P(None, ("dp", "sp")), P(None, ("dp", "sp")), P(), P(), P(), P(None, "dp"))
    out_specs = P(("dp", "sp"), None)
    return jax.shard_map(
        per_device, mesh=mesh, in_specs=in_specs, out_specs=out_specs, check_vma=False
    )
```

profile of v0, /device:TPU:0, one launch (start us, length us, event | category | flops | bytes accessed | tf_op | source)
XLA Modules:
  0.0 49.0 jit_solution(12381995538495456587)
XLA Ops:
  0.0 0.1 pad_add_fusion.1.place_ref
  0.1 2.7 %quarters.1 = (bf16[512,512]{1,0:T(8,128)(2,1)S(1)}, bf16[512,512]{1,0:T(8,128)(2,1)}) custom-call(s32[2]{0:T(128)S(1)} %pad_add_fusion.1.place_ref, bf16[2048,512]{1,0:T(8,128)(2,1)} %refs_0_.3), custom_call_target="tpu_custom_call" | custom-call | tf_op jit(solution)/shard_map/quarters/pallas_call | solution.py:196
  2.8 3.1 %collective-permute-start = (bf16[512,512]{1,0:T(8,128)(2,1)S(1)}, bf16[512,512]{1,0:T(8,128)(2,1)}, u32[]{:S(2)}, u32[]{:S(2)}) collective-permute-start(bf16[512,512]{1,0:T(8,128)(2,1)S(1)} %get-tuple-element.21), channel_id=1, source_target_pairs={{0,2},{1,3},{2,0},{3,1},{4,6},{5,7},{6,4},{7,5},{8,10},{9,11},{10,... | collective-permute-start | bytes 1572872 | tf_op jit(solution)/shard_map/ppermute | solution.py:277
  5.8 1.2 %glu.1 = (bf16[256,2048]{1,0:T(8,128)(2,1)S(1)}, bf16[16,2048]{1,0:T(8,128)(2,1)S(1)}, bf16[16,2048]{1,0:T(8,128)(2,1)S(1)}) custom-call(bf16[2048,256]{1,0:T(8,128)(2,1)S(1)} %copy-done.2, bf16[2048,256]{1,0:T(8,128)(2,1)S(1)} %copy-done.3), custom_call_target="tpu_custom_call" | custom-call | flops 10485760 | bytes 3145728 | tf_op jit(solution)/shard_map/glu/pallas_call | solution.py:36
  7.0 3.4 %collective-permute-start.4 = (bf16[16,2048]{1,0:T(8,128)(2,1)S(1)}, bf16[16,2048]{1,0:T(8,128)(2,1)S(1)}, u32[]{:S(2)}, u32[]{:S(2)}) collective-permute-start(bf16[16,2048]{1,0:T(8,128)(2,1)S(1)} %get-tuple-element.25), channel_id=1, source_target_pairs={{0,4},{4,8},{8,12},{12,16},{16,20},{20,24},{24,28},{1,5},{5,9},{9,... | collective-permute-start | bytes 196616 | tf_op jit(solution)/shard_map/ppermute | solution.py:282
  10.4 1.3 %collective-permute-start.5 = (bf16[16,2048]{1,0:T(8,128)(2,1)S(1)}, bf16[16,2048]{1,0:T(8,128)(2,1)S(1)}, u32[]{:S(2)}, u32[]{:S(2)}) collective-permute-start(bf16[16,2048]{1,0:T(8,128)(2,1)S(1)} %get-tuple-element.26), channel_id=1, source_target_pairs={{4,0},{8,4},{12,8},{16,12},{20,16},{24,20},{28,24},{5,1},{9,5},{13... | collective-permute-start | bytes 196616 | tf_op jit(solution)/shard_map/ppermute | solution.py:283
  11.7 6.8 %conv_inner.1._ = bf16[256,2048]{1,0:T(8,128)(2,1)S(1)} custom-call(bf16[256,2048]{1,0:T(8,128)(2,1)S(1)} %get-tuple-element.22.glu_ref, f32[31,2048]{1,0:T(8,128)S(1)} %copy-done.1, f32[1,2048]{1,0:T(1,128)S(1)} %bitcast.10, f32[1,2048]{1,0:T(1,128)S(1)} %bitcast.12), custom_call_target="tpu_custom_call" | custom-call | flops 41943040 | bytes 2097152 | tf_op jit(solution)/shard_map/conv_inner/pallas_call | solution.py:132
  18.6 0.0 copy-start
  18.6 1.4 %conv_outer.1.act_ref = bf16[256,2048]{1,0:T(8,128)(2,1)S(1)} custom-call(bf16[16,2048]{1,0:T(8,128)(2,1)S(1)} %collective-permute-done.4.before_ref, bf16[16,2048]{1,0:T(8,128)(2,1)S(1)} %collective-permute-done.5.after_ref, bf16[256,2048]{1,0:T(8,128)(2,1)S(1)} %get-tuple-element.22.glu_ref, ...), custom_call_target="tpu_custom_call", output_to_operand_aliasing={{}: (6, {})} | custom-call | flops 5242880 | bytes 262144 | tf_op jit(solution)/shard_map/conv_outer/pallas_call | solution.py:151
  20.0 0.1 collective-permute-start.6
  20.1 1.0 %collective-permute-start.3 = (bf16[512,512]{1,0:T(8,128)(2,1)}, bf16[512,512]{1,0:T(8,128)(2,1)}, u32[]{:S(2)}, u32[]{:S(2)}) collective-permute-start(bf16[512,512]{1,0:T(8,128)(2,1)} %get-tuple-element.24), channel_id=1, source_target_pairs={{0,2},{1,3},{2,0},{3,1},{4,6},{5,7},{6,4},{7,5},{8,10},{9,11},{10,... | collective-permute-start | bytes 1572872 | tf_op jit(solution)/shard_map/ppermute | solution.py:278
  21.1 3.2 %collective-permute-start.2 = (bf16[512,512]{1,0:T(8,128)(2,1)}, bf16[512,512]{1,0:T(8,128)(2,1)}, u32[]{:S(2)}, u32[]{:S(2)}) collective-permute-start(bf16[512,512]{1,0:T(8,128)(2,1)} %collective-permute-done.refs_0_), channel_id=1, source_target_pairs={{0,8},{4,12},{8,0},{12,4},{16,24},{20,28},{24,16},{28,20},{1,9},{5... | collective-permute-start | bytes 1572872 | tf_op jit(solution)/shard_map/ppermute | solution.py:271
  24.3 0.6 %collective-permute-start.1 = (bf16[512,512]{1,0:T(8,128)(2,1)}, bf16[512,512]{1,0:T(8,128)(2,1)}, u32[]{:S(2)}, u32[]{:S(2)}) collective-permute-start(bf16[512,512]{1,0:T(8,128)(2,1)} %collective-permute-done.refs_0_), channel_id=1, source_target_pairs={{0,4},{4,0},{8,12},{12,8},{16,20},{20,16},{24,28},{28,24},{1,5},{5... | collective-permute-start | bytes 1572872 | tf_op jit(solution)/shard_map/ppermute | solution.py:271
  24.9 0.1 pad_add_fusion.2.place_ref
  25.0 0.7 %project.4.refs_0_ = bf16[256,512]{1,0:T(8,128)(2,1)S(1)} custom-call(s32[1]{0:T(128)} %bitcast.4.place_ref, bf16[256,2048]{1,0:T(8,128)(2,1)S(1)} %conv_outer.1.act_ref, bf16[2048,512]{1,0:T(8,128)(2,1)S(1)} %copy-done), custom_call_target="tpu_custom_call" | custom-call | flops 536870912 | bytes 3145728 | tf_op jit(solution)/shard_map/project/pallas_call | solution.py:224
  25.7 9.1 %collective-permute-done.3.refs_1_ = bf16[512,512]{1,0:T(8,128)(2,1)} collective-permute-done((bf16[512,512]{1,0:T(8,128)(2,1)}, bf16[512,512]{1,0:T(8,128)(2,1)}, u32[]{:S(2)}, u32[]{:S(2)}) %collective-permute-start.3) | collective-permute-done | bytes 524320 | tf_op jit(solution)/shard_map/ppermute | solution.py:278
  34.8 2.1 %collective-permute-done.2.refs_3_ = bf16[512,512]{1,0:T(8,128)(2,1)} collective-permute-done((bf16[512,512]{1,0:T(8,128)(2,1)}, bf16[512,512]{1,0:T(8,128)(2,1)}, u32[]{:S(2)}, u32[]{:S(2)}) %collective-permute-start.2) | collective-permute-done | bytes 524320 | tf_op jit(solution)/shard_map/ppermute | solution.py:271
  36.9 1.5 %collective-permute-done.1.refs_2_ = bf16[512,512]{1,0:T(8,128)(2,1)} collective-permute-done((bf16[512,512]{1,0:T(8,128)(2,1)}, bf16[512,512]{1,0:T(8,128)(2,1)}, u32[]{:S(2)}, u32[]{:S(2)}) %collective-permute-start.1) | collective-permute-done | bytes 524320 | tf_op jit(solution)/shard_map/ppermute | solution.py:271
  38.3 3.3 %project.7 = bf16[256,512]{1,0:T(8,128)(2,1)} custom-call(s32[4]{0:T(128)S(1)} %pad_add_fusion.2.place_ref, bf16[256,2048]{1,0:T(8,128)(2,1)} %collective-permute-done.6.act_ref, bf16[512,512]{1,0:T(8,128)(2,1)} %collective-permute-done.refs_0_, bf16[512,512]{1,0:T(8,128)(2,1)} %collective-permute-done.3.refs_1_, ...), custom_call_target="tpu_custom_call" | custom-call | flops 536870912 | bytes 3145728 | tf_op jit(solution)/shard_map/project/pallas_call | solution.py:224
  41.6 2.6 %project.6 = bf16[256,512]{1,0:T(8,128)(2,1)} custom-call(s32[1]{0:T(128)} %bitcast.4.place_ref, bf16[256,2048]{1,0:T(8,128)(2,1)} %collective-permute-done.6.act_ref, bf16[2048,512]{1,0:T(8,128)(2,1)S(1)} %copy-done), custom_call_target="tpu_custom_call" | custom-call | flops 536870912 | bytes 3145728 | tf_op jit(solution)/shard_map/project/pallas_call | solution.py:224
  44.2 0.5 %collective-permute-start.7 = (bf16[256,512]{1,0:T(8,128)(2,1)}, bf16[256,512]{1,0:T(8,128)(2,1)S(1)}, u32[]{:S(2)}, u32[]{:S(2)}) collective-permute-start(bf16[256,512]{1,0:T(8,128)(2,1)} %project.6), channel_id=1, source_target_pairs={{0,1},{1,0},{2,3},{3,2},{4,5},{5,4},{6,7},{7,6},{8,9},{9,8},{10,11... | collective-permute-start | bytes 786440 | tf_op jit(solution)/shard_map/ppermute | solution.py:268
  44.7 0.1 pad_add_fusion.place_ref
  44.8 2.2 %project.5.refs_1_ = bf16[256,512]{1,0:T(8,128)(2,1)S(1)} custom-call(s32[4]{0:T(128)S(1)} %pad_add_fusion.2.place_ref, bf16[256,2048]{1,0:T(8,128)(2,1)S(1)} %conv_outer.1.act_ref, bf16[512,512]{1,0:T(8,128)(2,1)} %collective-permute-done.refs_0_, bf16[512,512]{1,0:T(8,128)(2,1)} %collective-permute-done.3.refs_1_, ...), custom_call_target="tpu_custom_call" | custom-call | flops 536870912 | bytes 3145728 | tf_op jit(solution)/shard_map/project/pallas_call | solution.py:224
  47.1 2.0 %collect.1 = bf16[256,2048]{1,0:T(8,128)(2,1)} custom-call(s32[4]{0:T(128)S(1)} %pad_add_fusion.place_ref, bf16[256,512]{1,0:T(8,128)(2,1)S(1)} %project.4.refs_0_, bf16[256,512]{1,0:T(8,128)(2,1)S(1)} %project.5.refs_1_, bf16[256,512]{1,0:T(8,128)(2,1)S(1)} %collective-permute-done.7.refs_2_, bf16[256,512]{1,0:T(8,128)(2,1)} %collective-permute-done.8.refs_3_), custom_call_target="tpu_custom_call" | custom-call | tf_op jit(solution)/shard_map/collect/pallas_call | solution.py:250
  (18 shorter events, 0.0 us)
Async XLA Ops:
  0.0 5.8 %copy-start.3 = (bf16[2048,256]{1,0:T(8,128)(2,1)S(1)}, bf16[2048,256]{1,0:T(8,128)(2,1)}, u32[]{:S(2)}) copy-start(bf16[2048,256]{1,0:T(8,128)(2,1)} %gate_ref.1) | copy-start | bytes 3145732
  0.0 5.8 %copy-start.2 = (bf16[2048,256]{1,0:T(8,128)(2,1)S(1)}, bf16[2048,256]{1,0:T(8,128)(2,1)}, u32[]{:S(2)}) copy-start(bf16[2048,256]{1,0:T(8,128)(2,1)} %lin_ref.1) | copy-start | bytes 3145732
  0.1 11.6 %copy-start.1 = (f32[31,2048]{1,0:T(8,128)S(1)}, f32[31,2048]{1,0:T(8,128)}, u32[]{:S(2)}) copy-start(f32[31,2048]{1,0:T(8,128)} %w_ref.5) | copy-start | bytes 761860
  0.1 11.6 %copy-start.4 = (f32[2048]{0:T(1024)S(1)}, f32[2048]{0:T(1024)}, u32[]{:S(2)}) copy-start(f32[2048]{0:T(1024)} %param.9) | copy-start | bytes 24580
  0.1 11.6 %copy-start.5 = (f32[2048]{0:T(1024)S(1)}, f32[2048]{0:T(1024)}, u32[]{:S(2)}) copy-start(f32[2048]{0:T(1024)} %param.10) | copy-start | bytes 24580
  2.8 15.8 %collective-permute-start = (bf16[512,512]{1,0:T(8,128)(2,1)S(1)}, bf16[512,512]{1,0:T(8,128)(2,1)}, u32[]{:S(2)}, u32[]{:S(2)}) collective-permute-start(bf16[512,512]{1,0:T(8,128)(2,1)S(1)} %get-tuple-element.21), channel_id=1, source_target_pairs={{0,2},{1,3},{2,0},{3,1},{4,6},{5,7},{6,4},{7,5},{8,10},{9,11},{10,... | collective-permute-start | bytes 1572872 | tf_op jit(solution)/shard_map/ppermute | solution.py:277
  7.0 11.6 %collective-permute-start.4 = (bf16[16,2048]{1,0:T(8,128)(2,1)S(1)}, bf16[16,2048]{1,0:T(8,128)(2,1)S(1)}, u32[]{:S(2)}, u32[]{:S(2)}) collective-permute-start(bf16[16,2048]{1,0:T(8,128)(2,1)S(1)} %get-tuple-element.25), channel_id=1, source_target_pairs={{0,4},{4,8},{8,12},{12,16},{16,20},{20,24},{24,28},{1,5},{5,9},{9,... | collective-permute-start | bytes 196616 | tf_op jit(solution)/shard_map/ppermute | solution.py:282
  10.4 8.2 %collective-permute-start.5 = (bf16[16,2048]{1,0:T(8,128)(2,1)S(1)}, bf16[16,2048]{1,0:T(8,128)(2,1)S(1)}, u32[]{:S(2)}, u32[]{:S(2)}) collective-permute-start(bf16[16,2048]{1,0:T(8,128)(2,1)S(1)} %get-tuple-element.26), channel_id=1, source_target_pairs={{4,0},{8,4},{12,8},{16,12},{20,16},{24,20},{28,24},{5,1},{9,5},{13... | collective-permute-start | bytes 196616 | tf_op jit(solution)/shard_map/ppermute | solution.py:283
  18.6 6.4 %copy-start = (bf16[2048,512]{1,0:T(8,128)(2,1)S(1)}, bf16[2048,512]{1,0:T(8,128)(2,1)}, u32[]{:S(2)}) copy-start(bf16[2048,512]{1,0:T(8,128)(2,1)} %refs_0_.3) | copy-start | bytes 6291460
  20.0 18.3 %collective-permute-start.6 = (bf16[256,2048]{1,0:T(8,128)(2,1)S(1)}, bf16[256,2048]{1,0:T(8,128)(2,1)}, u32[]{:S(2)}, u32[]{:S(2)}) collective-permute-start(bf16[256,2048]{1,0:T(8,128)(2,1)S(1)} %conv_outer.1.act_ref), channel_id=1, source_target_pairs={{0,1},{1,0},{2,3},{3,2},{4,5},{5,4},{6,7},{7,6},{8,9},{9,8},{10,11... | collective-permute-start | bytes 3145736 | tf_op jit(solution)/shard_map/ppermute | solution.py:268
  20.1 14.6 %collective-permute-start.3 = (bf16[512,512]{1,0:T(8,128)(2,1)}, bf16[512,512]{1,0:T(8,128)(2,1)}, u32[]{:S(2)}, u32[]{:S(2)}) collective-permute-start(bf16[512,512]{1,0:T(8,128)(2,1)} %get-tuple-element.24), channel_id=1, source_target_pairs={{0,2},{1,3},{2,0},{3,1},{4,6},{5,7},{6,4},{7,5},{8,10},{9,11},{10,... | collective-permute-start | bytes 1572872 | tf_op jit(solution)/shard_map/ppermute | solution.py:278
  21.1 15.7 %collective-permute-start.2 = (bf16[512,512]{1,0:T(8,128)(2,1)}, bf16[512,512]{1,0:T(8,128)(2,1)}, u32[]{:S(2)}, u32[]{:S(2)}) collective-permute-start(bf16[512,512]{1,0:T(8,128)(2,1)} %collective-permute-done.refs_0_), channel_id=1, source_target_pairs={{0,8},{4,12},{8,0},{12,4},{16,24},{20,28},{24,16},{28,20},{1,9},{5... | collective-permute-start | bytes 1572872 | tf_op jit(solution)/shard_map/ppermute | solution.py:271
  24.3 14.0 %collective-permute-start.1 = (bf16[512,512]{1,0:T(8,128)(2,1)}, bf16[512,512]{1,0:T(8,128)(2,1)}, u32[]{:S(2)}, u32[]{:S(2)}) collective-permute-start(bf16[512,512]{1,0:T(8,128)(2,1)} %collective-permute-done.refs_0_), channel_id=1, source_target_pairs={{0,4},{4,0},{8,12},{12,8},{16,20},{20,16},{24,28},{28,24},{1,5},{5... | collective-permute-start | bytes 1572872 | tf_op jit(solution)/shard_map/ppermute | solution.py:271
  41.6 5.5 %collective-permute-start.8 = (bf16[256,512]{1,0:T(8,128)(2,1)}, bf16[256,512]{1,0:T(8,128)(2,1)}, u32[]{:S(2)}, u32[]{:S(2)}) collective-permute-start(bf16[256,512]{1,0:T(8,128)(2,1)} %project.7), channel_id=1, source_target_pairs={{0,1},{1,0},{2,3},{3,2},{4,5},{5,4},{6,7},{7,6},{8,9},{9,8},{10,11... | collective-permute-start | bytes 786440 | tf_op jit(solution)/shard_map/ppermute | solution.py:268
  44.2 2.8 %collective-permute-start.7 = (bf16[256,512]{1,0:T(8,128)(2,1)}, bf16[256,512]{1,0:T(8,128)(2,1)S(1)}, u32[]{:S(2)}, u32[]{:S(2)}) collective-permute-start(bf16[256,512]{1,0:T(8,128)(2,1)} %project.6), channel_id=1, source_target_pairs={{0,1},{1,0},{2,3},{3,2},{4,5},{5,4},{6,7},{7,6},{8,9},{9,8},{10,11... | collective-permute-start | bytes 786440 | tf_op jit(solution)/shard_map/ppermute | solution.py:268
where the time goes:
time: 49.3 us; the launch traced here: 49 us
  Pallas kernels  22.8 us (46%)
  starting transfers between devices  13.1 us (27%)
  waiting for transfers between devices  12.6 us (26%)
    ppermute x1, waiting for transfers between devices, per_device(): direct_b = [lax.ppermute(second, 'dp', perm) for perm in hops]  9.06 us
    pallas_call x4, Pallas kernels, project(): pl.pallas_call(project_body, in_specs=[TABLE] + [WHOLE] * (1 + len(chunks...  8.81 us
    pallas_call x1, Pallas kernels, activated_inner(): pl.pallas_call(functools.partial(inner_body, tiles), out_shape=jax.ShapeD...  6.82 us
    ppermute x2, starting transfers between devices, to_near(): return lax.ppermute(x, 'sp', [(i, i ^ bit) for i in range(sp)])  3.76 us
    ppermute x2, waiting for transfers between devices, to_near(): return lax.ppermute(x, 'sp', [(i, i ^ bit) for i in range(sp)])  3.57 us
    ppermute x1, starting transfers between devices, per_device(): before = lax.ppermute(tail, 'sp', [(i, i + 1) for i in range(ends)])  3.4 us
    ppermute x1, starting transfers between devices, per_device(): direct_a = [lax.ppermute(first, 'dp', perm) for perm in hops]  3.06 us
    pallas_call x1, Pallas kernels, quarters(): pl.pallas_call(quarters_body, in_specs=[TABLE, STAY], out_specs=[WHOLE] *...  2.66 us
  transfers between devices with their start and end apart: 9, of which 3 were waited for; matrix products, arithmetic and copies ran while one was open for 0% of the time, Pallas kernels for 28%

commit v1 on v0

--- a/solution.py
+++ b/solution.py
@@ -14,7 +14,11 @@
 
 
 def params(semantics=None):
-    return pltpu.CompilerParams(dimension_semantics=semantics, vmem_limit_bytes=16 << 20)
+    return pltpu.CompilerParams(dimension_semantics=semantics, vmem_limit_bytes=8 << 20)
+
+
+def far_memory(x):
+    return pltpu.with_memory_space_constraint(x, pltpu.HBM)
 
 
 def cost(flops, nbytes):
@@ -178,47 +182,46 @@
 TABLE = pl.BlockSpec(memory_space=pltpu.SMEM)
 
 
-def quarters_body(place_ref, w_ref, *refs):
+def cut_body(place_ref, w_ref, *refs):
     outs, sems = refs[:-1], refs[-1]
-    rows = outs[0].shape[0]
-    copies = [
-        pltpu.make_async_copy(w_ref.at[pl.ds(place_ref[i] * rows, rows), :], out, sems.at[i])
-        for i, out in enumerate(outs)
-    ]
+    copies = []
+    for i, out in enumerate(outs):
+        start = pl.multiple_of(place_ref[i] * LANES, LANES)
+        rows = w_ref.at[pl.ds(start, out.shape[0]), :]
+        copies.append(pltpu.make_async_copy(rows, out, sems.at[i]))
     for copy in copies:
         copy.start()
     for copy in copies:
         copy.wait()
 
 
-def quarters(w_out, units):
-    shape = jax.ShapeDtypeStruct((w_out.shape[0] // 4, w_out.shape[1]), w_out.dtype)
-    return pl.pallas_call(
-        quarters_body,
+def cut(w_out, rows, places):
+    return pl.pallas_call(
+        cut_body,
         in_specs=[TABLE, STAY],
-        out_specs=[WHOLE] * len(units),
-        out_shape=[shape] * len(units),
-        scratch_shapes=[pltpu.SemaphoreType.DMA((len(units),))],
+        out_specs=[WHOLE] * len(places),
+        out_shape=[jax.ShapeDtypeStruct((rows, w_out.shape[1]), w_out.dtype)] * len(places),
+        scratch_shapes=[pltpu.SemaphoreType.DMA((len(places),))],
         compiler_params=params(),
-        name="quarters",
-    )(jnp.stack(units), pltpu.with_memory_space_constraint(w_out, pltpu.HBM))
+        name="cut",
+    )(jnp.stack(places), far_memory(w_out))
 
 
 def project_body(place_ref, act_ref, *refs):
     chunks, out_ref = refs[:-1], refs[-1]
-    rows = chunks[0].shape[0]
     total = None
     for i, chunk in enumerate(chunks):
         if len(chunks) == 1:
             part = act_ref[...]
         else:
-            part = act_ref[:, pl.ds(pl.multiple_of(place_ref[i] * rows, LANES), rows)]
+            start = pl.multiple_of(place_ref[i] * LANES, LANES)
+            part = act_ref[:, pl.ds(start, chunk.shape[0])]
         term = jnp.dot(part, chunk[...], preferred_element_type=jnp.float32)
         total = term if total is None else total + term
     out_ref[...] = total.astype(jnp.bfloat16)
 
 
-def project(act, chunks, units):
+def project(act, chunks, places):
     tokens, channels = act.shape
     width = chunks[0].shape[1]
     return pl.pallas_call(
@@ -229,7 +232,7 @@
         compiler_params=params(),
         cost_estimate=cost(2 * tokens * channels * width, 2 * channels * (tokens + width)),
         name="project",
-    )(jnp.stack(units), act, *chunks)
+    )(jnp.stack(places), act, *chunks)
 
 
 def collect_body(place_ref, *refs):
@@ -270,11 +273,20 @@
     def to_near(x, bit):
         return lax.ppermute(x, "sp", [(i, i ^ bit) for i in range(sp)])
 
-    first, second = quarters(w_out, (spot, 3 - spot))
+    quarter = w_out.shape[0] // 4
+    half = quarter // 2
+    tiles = quarter // LANES
+
+    def halves(unit):
+        return [unit * tiles, unit * tiles + tiles // 2]
+
     hops = [
         [(i, (i // 2 + k) % chips * 2 + i % 2) for i in range(dp)] for k in range(1, chips)
     ]
-    direct_a = [lax.ppermute(first, "dp", perm) for perm in hops]
+    firsts = cut(w_out, half, halves(spot))
+    direct_a1 = [lax.ppermute(firsts[0], "dp", perm) for perm in hops]
+    direct_a2 = [lax.ppermute(firsts[1], "dp", perm) for perm in hops]
+    (second,) = cut(w_out, quarter, ((3 - spot) * tiles,))
     direct_b = [lax.ppermute(second, "dp", perm) for perm in hops]
 
     glu, head, tail = gated(lin_pre, gate_pre)
@@ -283,25 +295,25 @@
     after = lax.ppermute(head, "sp", [(i + 1, i) for i in range(ends)])
     gain, shift = ln_gain[None, :], ln_shift[None, :]
     act = activated_inner(glu, w_depth, gain, shift)
-    direct_a, act = lax.optimization_barrier((direct_a, act))
-    by_x = [to_near(a, 1) for a in direct_a]
-    by_z = [to_near(a, 2) for a in direct_a]
+    by_x1 = [to_near(part, 1) for part in direct_a1]
+    by_z1 = [to_near(part, 2) for part in direct_a1]
+    direct_a2, act = lax.optimization_barrier((direct_a2, act))
+    by_x2 = [to_near(part, 1) for part in direct_a2]
+    by_z2 = [to_near(part, 2) for part in direct_a2]
     before, after, act = lax.optimization_barrier((before, after, act))
     act = activated_outer(before, after, glu, w_depth, gain, shift, act)
 
     act_far = to_sibling(act)
-    pieces, shards = [project(act, [w_out], (spot,))], [mine]
-    own_far = project(act_far, [w_out], (spot,))
+    pieces, shards = [project(act, [far_memory(w_out)], (spot,))], [mine]
+    own_far = project(act_far, [far_memory(w_out)], (spot,))
     received = [to_sibling(own_far)]
-    by_x, by_z, direct_b, act_far, act, pieces = lax.optimization_barrier(
-        (by_x, by_z, direct_b, act_far, act, pieces)
-    )
-    units = (spot, 3 - spot, spot ^ 1, spot ^ 2)
+    places = halves(spot) + [(3 - spot) * tiles] + halves(spot ^ 1) + halves(spot ^ 2)
+    arrivals = [direct_a1, direct_a2, direct_b, by_x1, by_x2, by_z1, by_z2]
     for k in range(1, chips):
-        near = [direct_a[k - 1], direct_b[k - 1], by_x[k - 1], by_z[k - 1]]
-        other_far = project(act_far, near, units)
+        near = [arrival[k - 1] for arrival in arrivals]
+        other_far = project(act_far, near, places)
         received.append(to_sibling(other_far))
-        pieces.append(project(act, near, units))
+        pieces.append(project(act, near, places))
         shards.append((mine // 2 - k) % chips * 2 + mine % 2)
     return collect(pieces + received, shards + [shard ^ 1 for shard in shards])
 

time: 49.3 us -> 53.3 us (1.081)
  the two profiles are of different devices: /device:TPU:0 before, /device:TPU:25 now
where the time goes in v1:
time: 53.3 us; the launch traced here: 53 us
  Pallas kernels  25.3 us (47%)
  waiting for transfers between devices  14.9 us (28%)
  starting transfers between devices  12.4 us (23%)
    pallas_call x4, Pallas kernels, project(): pl.pallas_call(project_body, in_specs=[TABLE] + [WHOLE] * (1 + len(chunks...  9.65 us
    ppermute x4, waiting for transfers between devices, to_near(): return lax.ppermute(x, 'sp', [(i, i ^ bit) for i in range(sp)])  7.96 us
    pallas_call x1, Pallas kernels, activated_inner(): pl.pallas_call(functools.partial(inner_body, tiles), out_shape=jax.ShapeD...  6.82 us
    ppermute x1, waiting for transfers between devices, per_device(): direct_a1 = [lax.ppermute(firsts[0], 'dp', perm) for perm in hops]  4.24 us
    pallas_call x2, Pallas kernels, cut(): pl.pallas_call(cut_body, in_specs=[TABLE, STAY], out_specs=[WHOLE] * len(...  4.23 us
    ppermute x1, starting transfers between devices, per_device(): before = lax.ppermute(tail, 'sp', [(i, i + 1) for i in range(ends)])  3.12 us
    ppermute x1, starting transfers between devices, per_device(): after = lax.ppermute(head, 'sp', [(i + 1, i) for i in range(ends)])  3.06 us
    ppermute x1, waiting for transfers between devices, per_device(): direct_b = [lax.ppermute(second, 'dp', perm) for perm in hops]  2.7 us
  transfers between devices with their start and end apart: 12, of which 5 were waited for; matrix products, arithmetic and copies ran while one was open for 0% of the time, Pallas kernels for 32%

profile of v1, /device:TPU:25, one launch (start us, length us, event | category | flops | bytes accessed | tf_op | source)
XLA Modules:
  0.0 53.0 jit_solution(11870258254470339900)
XLA Ops:
  0.1 2.4 %cut.2 = (bf16[256,512]{1,0:T(8,128)(2,1)}, bf16[256,512]{1,0:T(8,128)(2,1)S(1)}) custom-call(s32[2]{0:T(128)S(1)} %pad_add_fusion.1.place_ref, bf16[2048,512]{1,0:T(8,128)(2,1)} %refs_0_.3), custom_call_target="tpu_custom_call" | custom-call | tf_op jit(solution)/shard_map/cut/pallas_call | solution.py:199
  2.5 1.3 %collective-permute-start.2 = (bf16[256,512]{1,0:T(8,128)(2,1)S(1)}, bf16[256,512]{1,0:T(8,128)(2,1)S(1)}, u32[]{:S(2)}, u32[]{:S(2)}) collective-permute-start(bf16[256,512]{1,0:T(8,128)(2,1)S(1)} %get-tuple-element.17), channel_id=1, source_target_pairs={{0,2},{1,3},{2,0},{3,1},{4,6},{5,7},{6,4},{7,5},{8,10},{9,11},{10,... | collective-permute-start | bytes 786440 | tf_op jit(solution)/shard_map/ppermute | solution.py:288
  3.8 1.2 %glu.1 = (bf16[256,2048]{1,0:T(8,128)(2,1)S(1)}, bf16[16,2048]{1,0:T(8,128)(2,1)S(1)}, bf16[16,2048]{1,0:T(8,128)(2,1)S(1)}) custom-call(bf16[2048,256]{1,0:T(8,128)(2,1)S(1)} %copy-done.1, bf16[2048,256]{1,0:T(8,128)(2,1)S(1)} %copy-done.2), custom_call_target="tpu_custom_call" | custom-call | flops 10485760 | bytes 3145728 | tf_op jit(solution)/shard_map/glu/pallas_call | solution.py:40
  5.0 3.1 %collective-permute-start = (bf16[16,2048]{1,0:T(8,128)(2,1)S(1)}, bf16[16,2048]{1,0:T(8,128)(2,1)S(1)}, u32[]{:S(2)}, u32[]{:S(2)}) collective-permute-start(bf16[16,2048]{1,0:T(8,128)(2,1)S(1)} %get-tuple-element.15), channel_id=1, source_target_pairs={{0,4},{4,8},{8,12},{12,16},{16,20},{20,24},{24,28},{1,5},{5,9},{9,... | collective-permute-start | bytes 196616 | tf_op jit(solution)/shard_map/ppermute | solution.py:294
  8.1 3.1 %collective-permute-start.1 = (bf16[16,2048]{1,0:T(8,128)(2,1)S(1)}, bf16[16,2048]{1,0:T(8,128)(2,1)S(1)}, u32[]{:S(2)}, u32[]{:S(2)}) collective-permute-start(bf16[16,2048]{1,0:T(8,128)(2,1)S(1)} %get-tuple-element.16), channel_id=1, source_target_pairs={{4,0},{8,4},{12,8},{16,12},{20,16},{24,20},{28,24},{5,1},{9,5},{13... | collective-permute-start | bytes 196616 | tf_op jit(solution)/shard_map/ppermute | solution.py:295
  11.2 6.8 %conv_inner.1._ = bf16[256,2048]{1,0:T(8,128)(2,1)S(1)} custom-call(bf16[256,2048]{1,0:T(8,128)(2,1)S(1)} %get-tuple-element.18.glu_ref, f32[31,2048]{1,0:T(8,128)S(1)} %copy-done, f32[1,2048]{1,0:T(1,128)S(1)} %bitcast.14, f32[1,2048]{1,0:T(1,128)S(1)} %bitcast.16), custom_call_target="tpu_custom_call" | custom-call | flops 41943040 | bytes 2097152 | tf_op jit(solution)/shard_map/conv_inner/pallas_call | solution.py:136
  18.1 1.4 %conv_outer.1.act_ref = bf16[256,2048]{1,0:T(8,128)(2,1)S(1)} custom-call(bf16[16,2048]{1,0:T(8,128)(2,1)S(1)} %collective-permute-done.before_ref, bf16[16,2048]{1,0:T(8,128)(2,1)S(1)} %collective-permute-done.1.after_ref, bf16[256,2048]{1,0:T(8,128)(2,1)S(1)} %get-tuple-element.18.glu_ref, f32[31,2048]{1,0:T(8,128)S(1)} %copy-done, ...), custom_call_target="tpu_custom_call", output_to_operand_aliasing={{}: (6, {})} | custom-call | flops 5242880 | bytes 262144 | tf_op jit(solution)/shard_map/conv_outer/pallas_call | solution.py:155
  19.5 1.6 %collective-permute-start.9 = (bf16[256,2048]{1,0:T(8,128)(2,1)S(1)}, bf16[256,2048]{1,0:T(8,128)(2,1)S(1)}, u32[]{:S(2)}, u32[]{:S(2)}) collective-permute-start(bf16[256,2048]{1,0:T(8,128)(2,1)S(1)} %conv_outer.1.act_ref), channel_id=1, source_target_pairs={{0,1},{1,0},{2,3},{3,2},{4,5},{5,4},{6,7},{7,6},{8,9},{9,8},{10,11... | collective-permute-start | bytes 3145736 | tf_op jit(solution)/shard_map/ppermute | solution.py:271
  21.1 0.2 collective-permute-start.3
  21.3 0.3 collective-permute-start.6
  21.6 1.8 %cut.3 = bf16[512,512]{1,0:T(8,128)(2,1)} custom-call(s32[1]{0:T(128)} %bitcast.9.place_ref, bf16[2048,512]{1,0:T(8,128)(2,1)} %refs_0_.3), custom_call_target="tpu_custom_call" | custom-call | tf_op jit(solution)/shard_map/cut/pallas_call | solution.py:199
  23.5 1.3 %collective-permute-start.4 = (bf16[512,512]{1,0:T(8,128)(2,1)}, bf16[512,512]{1,0:T(8,128)(2,1)S(1)}, u32[]{:S(2)}, u32[]{:S(2)}) collective-permute-start(bf16[512,512]{1,0:T(8,128)(2,1)} %cut.3), channel_id=1, source_target_pairs={{0,2},{1,3},{2,0},{3,1},{4,6},{5,7},{6,4},{7,5},{8,10},{9,11},{10,... | collective-permute-start | bytes 1572872 | tf_op jit(solution)/shard_map/ppermute | solution.py:290
  24.9 4.2 %collective-permute-done.3.refs_0_ = bf16[256,512]{1,0:T(8,128)(2,1)S(1)} collective-permute-done((bf16[256,512]{1,0:T(8,128)(2,1)}, bf16[256,512]{1,0:T(8,128)(2,1)S(1)}, u32[]{:S(2)}, u32[]{:S(2)}) %collective-permute-start.3) | collective-permute-done | bytes 262176 | tf_op jit(solution)/shard_map/ppermute | solution.py:287
  29.2 0.2 collective-permute-start.5
  29.6 2.2 %collective-permute-done.8.refs_6_ = bf16[256,512]{1,0:T(8,128)(2,1)} collective-permute-done((bf16[256,512]{1,0:T(8,128)(2,1)S(1)}, bf16[256,512]{1,0:T(8,128)(2,1)}, u32[]{:S(2)}, u32[]{:S(2)}) %collective-permute-start.8) | collective-permute-done | bytes 262176 | tf_op jit(solution)/shard_map/ppermute | solution.py:274
  31.8 4.0 %collective-permute-done.5.refs_3_ = bf16[256,512]{1,0:T(8,128)(2,1)} collective-permute-done((bf16[256,512]{1,0:T(8,128)(2,1)S(1)}, bf16[256,512]{1,0:T(8,128)(2,1)}, u32[]{:S(2)}, u32[]{:S(2)}) %collective-permute-start.5) | collective-permute-done | bytes 262176 | tf_op jit(solution)/shard_map/ppermute | solution.py:274
  35.8 1.8 %collective-permute-done.7.refs_5_ = bf16[256,512]{1,0:T(8,128)(2,1)} collective-permute-done((bf16[256,512]{1,0:T(8,128)(2,1)S(1)}, bf16[256,512]{1,0:T(8,128)(2,1)}, u32[]{:S(2)}, u32[]{:S(2)}) %collective-permute-start.7) | collective-permute-done | bytes 262176 | tf_op jit(solution)/shard_map/ppermute | solution.py:274
  37.6 2.7 %collective-permute-done.4.refs_2_ = bf16[512,512]{1,0:T(8,128)(2,1)S(1)} collective-permute-done((bf16[512,512]{1,0:T(8,128)(2,1)}, bf16[512,512]{1,0:T(8,128)(2,1)S(1)}, u32[]{:S(2)}, u32[]{:S(2)}) %collective-permute-start.4) | collective-permute-done | bytes 524320 | tf_op jit(solution)/shard_map/ppermute | solution.py:290
  40.3 2.5 %project.7 = bf16[256,512]{1,0:T(8,128)(2,1)} custom-call(s32[7]{0:T(128)S(1)} %stack.71.place_ref, bf16[256,2048]{1,0:T(8,128)(2,1)S(1)} %collective-permute-done.9.act_ref, bf16[256,512]{1,0:T(8,128)(2,1)S(1)} %collective-permute-done.3.refs_0_, bf16[256,512]{1,0:T(8,128)(2,1)S(1)} %collective-permute-done.2.refs_1_, ...), custom_call_target="tpu_custom_call" | custom-call | flops 536870912 | bytes 3145728 | tf_op jit(solution)/shard_map/project/pallas_call | solution.py:227
  42.8 0.9 %collective-permute-start.11 = (bf16[256,512]{1,0:T(8,128)(2,1)}, bf16[256,512]{1,0:T(8,128)(2,1)}, u32[]{:S(2)}, u32[]{:S(2)}) collective-permute-start(bf16[256,512]{1,0:T(8,128)(2,1)} %project.7), channel_id=1, source_target_pairs={{0,1},{1,0},{2,3},{3,2},{4,5},{5,4},{6,7},{7,6},{8,9},{9,8},{10,11... | collective-permute-start | bytes 786440 | tf_op jit(solution)/shard_map/ppermute | solution.py:271
  43.8 3.0 %project.6 = bf16[256,512]{1,0:T(8,128)(2,1)} custom-call(s32[1]{0:T(128)} %bitcast.4.place_ref, bf16[256,2048]{1,0:T(8,128)(2,1)S(1)} %collective-permute-done.9.act_ref, bf16[2048,512]{1,0:T(8,128)(2,1)} %refs_0_.3), custom_call_target="tpu_custom_call" | custom-call | flops 536870912 | bytes 3145728 | tf_op jit(solution)/shard_map/project/pallas_call | solution.py:227
  46.9 2.3 %project.4.refs_0_ = bf16[256,512]{1,0:T(8,128)(2,1)S(1)} custom-call(s32[1]{0:T(128)} %bitcast.4.place_ref, bf16[256,2048]{1,0:T(8,128)(2,1)S(1)} %conv_outer.1.act_ref, bf16[2048,512]{1,0:T(8,128)(2,1)} %refs_0_.3), custom_call_target="tpu_custom_call" | custom-call | flops 536870912 | bytes 3145728 | tf_op jit(solution)/shard_map/project/pallas_call | solution.py:227
  49.2 1.8 %project.5.refs_1_ = bf16[256,512]{1,0:T(8,128)(2,1)S(1)} custom-call(s32[7]{0:T(128)S(1)} %stack.71.place_ref, bf16[256,2048]{1,0:T(8,128)(2,1)S(1)} %conv_outer.1.act_ref, bf16[256,512]{1,0:T(8,128)(2,1)S(1)} %collective-permute-done.3.refs_0_, bf16[256,512]{1,0:T(8,128)(2,1)S(1)} %collective-permute-done.2.refs_1_, ...), custom_call_target="tpu_custom_call" | custom-call | flops 536870912 | bytes 3145728 | tf_op jit(solution)/shard_map/project/pallas_call | solution.py:227
  51.0 2.0 %collect.1 = bf16[256,2048]{1,0:T(8,128)(2,1)} custom-call(s32[4]{0:T(128)S(1)} %pad_add_fusion.place_ref, bf16[256,512]{1,0:T(8,128)(2,1)S(1)} %project.4.refs_0_, bf16[256,512]{1,0:T(8,128)(2,1)S(1)} %project.5.refs_1_, bf16[256,512]{1,0:T(8,128)(2,1)S(1)} %collective-permute-done.10.refs_2_, bf16[256,512]{1,0:T(8,128)(2,1)} %collective-permute-done.11.refs_3_), custom_call_target="tpu_custom_call" | custom-call | tf_op jit(solution)/shard_map/collect/pallas_call | solution.py:253
  (23 shorter events, 0.6 us)
Async XLA Ops:
  0.0 3.8 %copy-start.1 = (bf16[2048,256]{1,0:T(8,128)(2,1)S(1)}, bf16[2048,256]{1,0:T(8,128)(2,1)}, u32[]{:S(2)}) copy-start(bf16[2048,256]{1,0:T(8,128)(2,1)} %lin_ref.1) | copy-start | bytes 3145732
  0.0 3.8 %copy-start.2 = (bf16[2048,256]{1,0:T(8,128)(2,1)S(1)}, bf16[2048,256]{1,0:T(8,128)(2,1)}, u32[]{:S(2)}) copy-start(bf16[2048,256]{1,0:T(8,128)(2,1)} %gate_ref.1) | copy-start | bytes 3145732
  0.1 11.1 %copy-start = (f32[31,2048]{1,0:T(8,128)S(1)}, f32[31,2048]{1,0:T(8,128)}, u32[]{:S(2)}) copy-start(f32[31,2048]{1,0:T(8,128)} %w_ref.6) | copy-start | bytes 761860
  0.1 11.1 %copy-start.3 = (f32[2048]{0:T(1024)S(1)}, f32[2048]{0:T(1024)}, u32[]{:S(2)}) copy-start(f32[2048]{0:T(1024)} %param.9) | copy-start | bytes 24580
  0.1 11.1 %copy-start.4 = (f32[2048]{0:T(1024)S(1)}, f32[2048]{0:T(1024)}, u32[]{:S(2)}) copy-start(f32[2048]{0:T(1024)} %param.10) | copy-start | bytes 24580
  2.5 15.5 %collective-permute-start.2 = (bf16[256,512]{1,0:T(8,128)(2,1)S(1)}, bf16[256,512]{1,0:T(8,128)(2,1)S(1)}, u32[]{:S(2)}, u32[]{:S(2)}) collective-permute-start(bf16[256,512]{1,0:T(8,128)(2,1)S(1)} %get-tuple-element.17), channel_id=1, source_target_pairs={{0,2},{1,3},{2,0},{3,1},{4,6},{5,7},{6,4},{7,5},{8,10},{9,11},{10,... | collective-permute-start | bytes 786440 | tf_op jit(solution)/shard_map/ppermute | solution.py:288
  5.0 13.1 %collective-permute-start = (bf16[16,2048]{1,0:T(8,128)(2,1)S(1)}, bf16[16,2048]{1,0:T(8,128)(2,1)S(1)}, u32[]{:S(2)}, u32[]{:S(2)}) collective-permute-start(bf16[16,2048]{1,0:T(8,128)(2,1)S(1)} %get-tuple-element.15), channel_id=1, source_target_pairs={{0,4},{4,8},{8,12},{12,16},{16,20},{20,24},{24,28},{1,5},{5,9},{9,... | collective-permute-start | bytes 196616 | tf_op jit(solution)/shard_map/ppermute | solution.py:294
  8.1 9.9 %collective-permute-start.1 = (bf16[16,2048]{1,0:T(8,128)(2,1)S(1)}, bf16[16,2048]{1,0:T(8,128)(2,1)S(1)}, u32[]{:S(2)}, u32[]{:S(2)}) collective-permute-start(bf16[16,2048]{1,0:T(8,128)(2,1)S(1)} %get-tuple-element.16), channel_id=1, source_target_pairs={{4,0},{8,4},{12,8},{16,12},{20,16},{24,20},{28,24},{5,1},{9,5},{13... | collective-permute-start | bytes 196616 | tf_op jit(solution)/shard_map/ppermute | solution.py:295
  19.5 20.8 %collective-permute-start.9 = (bf16[256,2048]{1,0:T(8,128)(2,1)S(1)}, bf16[256,2048]{1,0:T(8,128)(2,1)S(1)}, u32[]{:S(2)}, u32[]{:S(2)}) collective-permute-start(bf16[256,2048]{1,0:T(8,128)(2,1)S(1)} %conv_outer.1.act_ref), channel_id=1, source_target_pairs={{0,1},{1,0},{2,3},{3,2},{4,5},{5,4},{6,7},{7,6},{8,9},{9,8},{10,11... | collective-permute-start | bytes 3145736 | tf_op jit(solution)/shard_map/ppermute | solution.py:271
  21.1 8.1 %collective-permute-start.3 = (bf16[256,512]{1,0:T(8,128)(2,1)}, bf16[256,512]{1,0:T(8,128)(2,1)S(1)}, u32[]{:S(2)}, u32[]{:S(2)}) collective-permute-start(bf16[256,512]{1,0:T(8,128)(2,1)} %get-tuple-element.23), channel_id=1, source_target_pairs={{0,2},{1,3},{2,0},{3,1},{4,6},{5,7},{6,4},{7,5},{8,10},{9,11},{10,... | collective-permute-start | bytes 786440 | tf_op jit(solution)/shard_map/ppermute | solution.py:287
  21.3 8.1 %collective-permute-start.6 = (bf16[256,512]{1,0:T(8,128)(2,1)S(1)}, bf16[256,512]{1,0:T(8,128)(2,1)S(1)}, u32[]{:S(2)}, u32[]{:S(2)}) collective-permute-start(bf16[256,512]{1,0:T(8,128)(2,1)S(1)} %collective-permute-done.2.refs_1_), channel_id=1, source_target_pairs={{0,4},{4,0},{8,12},{12,8},{16,20},{20,16},{24,28},{28,24},{1,5},{5... | collective-permute-start | bytes 786440 | tf_op jit(solution)/shard_map/ppermute | solution.py:274
  23.5 16.8 %collective-permute-start.4 = (bf16[512,512]{1,0:T(8,128)(2,1)}, bf16[512,512]{1,0:T(8,128)(2,1)S(1)}, u32[]{:S(2)}, u32[]{:S(2)}) collective-permute-start(bf16[512,512]{1,0:T(8,128)(2,1)} %cut.3), channel_id=1, source_target_pairs={{0,2},{1,3},{2,0},{3,1},{4,6},{5,7},{6,4},{7,5},{8,10},{9,11},{10,... | collective-permute-start | bytes 1572872 | tf_op jit(solution)/shard_map/ppermute | solution.py:290
  24.8 7.0 %collective-permute-start.8 = (bf16[256,512]{1,0:T(8,128)(2,1)S(1)}, bf16[256,512]{1,0:T(8,128)(2,1)}, u32[]{:S(2)}, u32[]{:S(2)}) collective-permute-start(bf16[256,512]{1,0:T(8,128)(2,1)S(1)} %collective-permute-done.2.refs_1_), channel_id=1, source_target_pairs={{0,8},{4,12},{8,0},{12,4},{16,24},{20,28},{24,16},{28,20},{1,9},{5... | collective-permute-start | bytes 786440 | tf_op jit(solution)/shard_map/ppermute | solution.py:274
  29.2 6.6 %collective-permute-start.5 = (bf16[256,512]{1,0:T(8,128)(2,1)S(1)}, bf16[256,512]{1,0:T(8,128)(2,1)}, u32[]{:S(2)}, u32[]{:S(2)}) collective-permute-start(bf16[256,512]{1,0:T(8,128)(2,1)S(1)} %collective-permute-done.3.refs_0_), channel_id=1, source_target_pairs={{0,4},{4,0},{8,12},{12,8},{16,20},{20,16},{24,28},{28,24},{1,5},{5... | collective-permute-start | bytes 786440 | tf_op jit(solution)/shard_map/ppermute | solution.py:274
  29.4 8.2 %collective-permute-start.7 = (bf16[256,512]{1,0:T(8,128)(2,1)S(1)}, bf16[256,512]{1,0:T(8,128)(2,1)}, u32[]{:S(2)}, u32[]{:S(2)}) collective-permute-start(bf16[256,512]{1,0:T(8,128)(2,1)S(1)} %collective-permute-done.3.refs_0_), channel_id=1, source_target_pairs={{0,8},{4,12},{8,0},{12,4},{16,24},{20,28},{24,16},{28,20},{1,9},{5... | collective-permute-start | bytes 786440 | tf_op jit(solution)/shard_map/ppermute | solution.py:274
  42.8 8.2 %collective-permute-start.11 = (bf16[256,512]{1,0:T(8,128)(2,1)}, bf16[256,512]{1,0:T(8,128)(2,1)}, u32[]{:S(2)}, u32[]{:S(2)}) collective-permute-start(bf16[256,512]{1,0:T(8,128)(2,1)} %project.7), channel_id=1, source_target_pairs={{0,1},{1,0},{2,3},{3,2},{4,5},{5,4},{6,7},{7,6},{8,9},{9,8},{10,11... | collective-permute-start | bytes 786440 | tf_op jit(solution)/shard_map/ppermute | solution.py:271
  46.8 4.2 %collective-permute-start.10 = (bf16[256,512]{1,0:T(8,128)(2,1)}, bf16[256,512]{1,0:T(8,128)(2,1)S(1)}, u32[]{:S(2)}, u32[]{:S(2)}) collective-permute-start(bf16[256,512]{1,0:T(8,128)(2,1)} %project.6), channel_id=1, source_target_pairs={{0,1},{1,0},{2,3},{3,2},{4,5},{5,4},{6,7},{7,6},{8,9},{9,8},{10,11... | collective-permute-start | bytes 786440 | tf_op jit(solution)/shard_map/ppermute | solution.py:271

commit v2 on v1

--- a/solution.py
+++ b/solution.py
@@ -11,6 +11,9 @@
 LANES = 128
 EDGE = 16
 EPS = 1e-05
+WHOLE = pl.BlockSpec(memory_space=pltpu.VMEM)
+STAY = pl.BlockSpec(memory_space=pltpu.HBM)
+TABLE = pl.BlockSpec(memory_space=pltpu.SMEM)
 
 
 def params(semantics=None):
@@ -25,22 +28,24 @@
     return pl.CostEstimate(flops=flops, transcendentals=0, bytes_accessed=nbytes)
 
 
-def glu_body(lin_ref, gate_ref, out_ref, head_ref, tail_ref):
+def glu_body(parity_ref, lin_ref, gate_ref, out_ref, near_ref, next_ref):
     gate = gate_ref[...].astype(jnp.float32)
     glu = (lin_ref[...].astype(jnp.float32) * jax.nn.sigmoid(gate)).T.astype(jnp.bfloat16)
     out_ref[...] = glu
-    head_ref[...] = glu[:EDGE]
-    tail_ref[...] = glu[glu.shape[0] - EDGE :]
-
-
-def gated(lin_pre, gate_pre):
+    head, tail = glu[:EDGE], glu[glu.shape[0] - EDGE :]
+    even = parity_ref[0] == 0
+    near_ref[...] = jnp.where(even, tail, head)
+    next_ref[...] = jnp.where(even, head, tail)
+
+
+def gated(parity, lin_pre, gate_pre):
     channels, tokens = lin_pre.shape
     block = 256
     edge = pl.BlockSpec((EDGE, block), lambda i: (0, i))
     return pl.pallas_call(
         glu_body,
         grid=(channels // block,),
-        in_specs=[pl.BlockSpec((block, tokens), lambda i: (i, 0))] * 2,
+        in_specs=[TABLE] + [pl.BlockSpec((block, tokens), lambda i: (i, 0))] * 2,
         out_specs=[pl.BlockSpec((tokens, block), lambda i: (0, i)), edge, edge],
         out_shape=[
             jax.ShapeDtypeStruct((tokens, channels), jnp.bfloat16),
@@ -50,7 +55,7 @@
         compiler_params=params(("arbitrary",)),
         cost_estimate=cost(20 * channels * tokens, 6 * channels * tokens),
         name="glu",
-    )(lin_pre, gate_pre)
+    )(parity, lin_pre, gate_pre)
 
 
 def conv_norm(cells, w_ref, gain_ref, shift_ref, mixed, start, tiles, store):
@@ -110,13 +115,14 @@
     lax.fori_loop(0, (glu_ref.shape[0] - 2 * EDGE) // span, chunk, 0)
 
 
-def outer_body(before_ref, after_ref, glu_ref, w_ref, gain_ref, shift_ref, _, out_ref, cells, mixed):
+def outer_body(parity_ref, near_ref, next_ref, glu_ref, w_ref, gain_ref, shift_ref, _, out_ref, cells, mixed):
     side = pl.program_id(0)
     blocks = cells.shape[0]
     for block in range(blocks):
         lanes = pl.ds(block * LANES, LANES)
         own = glu_ref[:, lanes].astype(jnp.float32)
-        halo = jnp.where(side == 0, before_ref[:, lanes], after_ref[:, lanes]).astype(jnp.float32)
+        halo = jnp.where(side != parity_ref[0], near_ref[:, lanes], next_ref[:, lanes])
+        halo = halo.astype(jnp.float32)
         cells[block, pl.ds(EDGE, 2 * EDGE), :] = jnp.where(side == 0, own, 0.0)
         cells[block, pl.ds(0, EDGE), :] = jnp.where(side == 0, halo, own[:EDGE])
         cells[block, pl.ds(EDGE, EDGE), :] = jnp.where(side == 0, own[:EDGE], own[EDGE:])
@@ -146,7 +152,7 @@
     )(glu, w_depth, gain, shift)
 
 
-def activated_outer(before, after, glu, w_depth, gain, shift, act):
+def activated_outer(parity, near, ahead, glu, w_depth, gain, shift, act):
     tokens, channels = glu.shape
     blocks = channels // LANES
     whole = pl.BlockSpec((EDGE, channels), lambda i: (0, 0))
@@ -156,6 +162,7 @@
         outer_body,
         grid=(2,),
         in_specs=[
+            TABLE,
             whole,
             whole,
             pl.BlockSpec((2 * EDGE, channels), lambda i: (i * (tokens // (2 * EDGE) - 1), 0)),
@@ -170,16 +177,11 @@
             pltpu.VMEM((blocks, 3 * EDGE, LANES), jnp.float32),
             pltpu.VMEM((blocks, EDGE, LANES), jnp.float32),
         ],
-        input_output_aliases={6: 0},
+        input_output_aliases={7: 0},
         compiler_params=params(("arbitrary",)),
         cost_estimate=cost(80 * channels * 2 * EDGE, 8 * channels * EDGE),
         name="conv_outer",
-    )(before, after, glu, w_depth, gain, shift, act)
-
-
-WHOLE = pl.BlockSpec(memory_space=pltpu.VMEM)
-STAY = pl.BlockSpec(memory_space=pltpu.HBM)
-TABLE = pl.BlockSpec(memory_space=pltpu.SMEM)
+    )(parity, near, ahead, glu, w_depth, gain, shift, act)
 
 
 def cut_body(place_ref, w_ref, *refs):
@@ -207,36 +209,63 @@
     )(jnp.stack(places), far_memory(w_out))
 
 
-def project_body(place_ref, act_ref, *refs):
-    chunks, out_ref = refs[:-1], refs[-1]
-    total = None
-    for i, chunk in enumerate(chunks):
-        if len(chunks) == 1:
-            part = act_ref[...]
-        else:
-            start = pl.multiple_of(place_ref[i] * LANES, LANES)
-            part = act_ref[:, pl.ds(start, chunk.shape[0])]
-        term = jnp.dot(part, chunk[...], preferred_element_type=jnp.float32)
-        total = term if total is None else total + term
-    out_ref[...] = total.astype(jnp.bfloat16)
-
-
-def project(act, chunks, places):
-    tokens, channels = act.shape
+def project_body(count, place_ref, far_ref, near_ref, *refs):
+    for act_ref, out_ref in zip((far_ref, near_ref), refs[-2:]):
+        total = None
+        for i, chunk in enumerate(refs[:count]):
+            if count == 1:
+                part = act_ref[...]
+            else:
+                start = pl.multiple_of(place_ref[i] * LANES, LANES)
+                part = act_ref[:, pl.ds(start, chunk.shape[0])]
+            term = jnp.dot(part, chunk[...], preferred_element_type=jnp.float32)
+            total = term if total is None else total + term
+        out_ref[...] = total.astype(jnp.bfloat16)
+
+
+def project(far, near, chunks, places, shard, columns, out):
+    tokens, channels = near.shape
     width = chunks[0].shape[1]
-    return pl.pallas_call(
-        project_body,
-        in_specs=[TABLE] + [WHOLE] * (1 + len(chunks)),
-        out_specs=WHOLE,
-        out_shape=jax.ShapeDtypeStruct((tokens, width), jnp.bfloat16),
-        compiler_params=params(),
-        cost_estimate=cost(2 * tokens * channels * width, 2 * channels * (tokens + width)),
+    block = min(width, 256)
+    steps = width // block
+    act_spec = pl.BlockSpec((tokens, channels), lambda i, place: (0, 0))
+    in_specs = [act_spec] * 2
+    in_specs += [pl.BlockSpec((chunk.shape[0], block), lambda i, place: (0, i)) for chunk in chunks]
+    operands = [far, near, *chunks]
+    aliases = {}
+    if out is not None:
+        aliases = {len(operands) + 1: 1}
+        in_specs.append(STAY)
+        operands.append(out)
+    flops = 4 * tokens * channels * width
+    return pl.pallas_call(
+        functools.partial(project_body, len(chunks)),
+        grid_spec=pltpu.PrefetchScalarGridSpec(
+            num_scalar_prefetch=1,
+            grid=(steps,),
+            in_specs=in_specs,
+            out_specs=[
+                pl.BlockSpec((tokens, block), lambda i, place: (0, i)),
+                pl.BlockSpec(
+                    (tokens, block), lambda i, place: (0, place[len(places)] * steps + i)
+                ),
+            ],
+        ),
+        out_shape=[
+            jax.ShapeDtypeStruct((tokens, width), jnp.bfloat16),
+            pltpu.HBM((tokens, columns), jnp.bfloat16),
+        ],
+        input_output_aliases=aliases,
+        compiler_params=pltpu.CompilerParams(
+            dimension_semantics=("arbitrary",), vmem_limit_bytes=16 << 20
+        ),
+        cost_estimate=cost(flops, 2 * channels * (2 * tokens + width)),
         name="project",
-    )(jnp.stack(places), act, *chunks)
+    )(jnp.stack([*places, shard]), *operands)
 
 
 def collect_body(place_ref, *refs):
-    pieces, out_ref, sems = refs[:-2], refs[-2], refs[-1]
+    pieces, out_ref, sems = refs[:-3], refs[-2], refs[-1]
     width = pieces[0].shape[1]
     copies = []
     for i, piece in enumerate(pieces):
@@ -248,24 +277,26 @@
         copy.wait()
 
 
-def collect(pieces, shards):
-    tokens, width = pieces[0].shape
+def collect(pieces, shards, out):
     return pl.pallas_call(
         collect_body,
-        in_specs=[TABLE] + [WHOLE] * len(pieces),
+        in_specs=[TABLE] + [WHOLE] * len(pieces) + [STAY],
         out_specs=STAY,
-        out_shape=jax.ShapeDtypeStruct((tokens, width * len(pieces)), jnp.bfloat16),
+        out_shape=jax.ShapeDtypeStruct(out.shape, out.dtype),
         scratch_shapes=[pltpu.SemaphoreType.DMA((len(pieces),))],
+        input_output_aliases={1 + len(pieces): 0},
         compiler_params=params(),
         name="collect",
-    )(jnp.stack(shards), *pieces)
+    )(jnp.stack(shards), *pieces, out)
 
 
 def per_device(lin_pre, gate_pre, w_depth, ln_gain, ln_shift, w_out):
     dp, sp = lax.axis_size("dp"), lax.axis_size("sp")
     chips = dp // 2
-    mine = lax.axis_index("dp")
-    spot = lax.axis_index("sp") % 4
+    mine, place = lax.axis_index("dp"), lax.axis_index("sp")
+    spot = place % 4
+    parity = (place % 2)[None]
+    tiles = w_out.shape[0] // 4 // LANES
 
     def to_sibling(x):
         return lax.ppermute(x, "dp", [(i, i ^ 1) for i in range(dp)])
@@ -273,49 +304,38 @@
     def to_near(x, bit):
         return lax.ppermute(x, "sp", [(i, i ^ bit) for i in range(sp)])
 
-    quarter = w_out.shape[0] // 4
-    half = quarter // 2
-    tiles = quarter // LANES
-
-    def halves(unit):
-        return [unit * tiles, unit * tiles + tiles // 2]
-
+    places = [unit * tiles for unit in (spot, 3 - spot, spot ^ 1, spot ^ 2)]
+    first, second = cut(w_out, w_out.shape[0] // 4, places[:2])
     hops = [
         [(i, (i // 2 + k) % chips * 2 + i % 2) for i in range(dp)] for k in range(1, chips)
     ]
-    firsts = cut(w_out, half, halves(spot))
-    direct_a1 = [lax.ppermute(firsts[0], "dp", perm) for perm in hops]
-    direct_a2 = [lax.ppermute(firsts[1], "dp", perm) for perm in hops]
-    (second,) = cut(w_out, quarter, ((3 - spot) * tiles,))
+    direct_a = [lax.ppermute(first, "dp", perm) for perm in hops]
     direct_b = [lax.ppermute(second, "dp", perm) for perm in hops]
 
-    glu, head, tail = gated(lin_pre, gate_pre)
-    ends = sp - 1
-    before = lax.ppermute(tail, "sp", [(i, i + 1) for i in range(ends)])
-    after = lax.ppermute(head, "sp", [(i + 1, i) for i in range(ends)])
+    glu, to_pair, to_next = gated(parity, far_memory(lin_pre), far_memory(gate_pre))
+    odd = [(i, i + 1) for i in range(1, sp - 1, 2)]
+    from_pair = to_near(to_pair, 1)
+    from_next = lax.ppermute(to_next, "sp", odd + [(j, i) for i, j in odd])
     gain, shift = ln_gain[None, :], ln_shift[None, :]
     act = activated_inner(glu, w_depth, gain, shift)
-    by_x1 = [to_near(part, 1) for part in direct_a1]
-    by_z1 = [to_near(part, 2) for part in direct_a1]
-    direct_a2, act = lax.optimization_barrier((direct_a2, act))
-    by_x2 = [to_near(part, 1) for part in direct_a2]
-    by_z2 = [to_near(part, 2) for part in direct_a2]
-    before, after, act = lax.optimization_barrier((before, after, act))
-    act = activated_outer(before, after, glu, w_depth, gain, shift, act)
+    direct_a, act = lax.optimization_barrier((direct_a, act))
+    by_x = [to_near(part, 1) for part in direct_a]
+    by_z = [to_near(part, 2) for part in direct_a]
+    from_pair, from_next, act = lax.optimization_barrier((from_pair, from_next, act))
+    act = activated_outer(parity, from_pair, from_next, glu, w_depth, gain, shift, act)
 
     act_far = to_sibling(act)
-    pieces, shards = [project(act, [far_memory(w_out)], (spot,))], [mine]
-    own_far = project(act_far, [far_memory(w_out)], (spot,))
+    columns = w_out.shape[1] * dp
+    own_far, out = project(act_far, act, [far_memory(w_out)], places[:1], mine, columns, None)
+    shards = [mine ^ 1]
     received = [to_sibling(own_far)]
-    places = halves(spot) + [(3 - spot) * tiles] + halves(spot ^ 1) + halves(spot ^ 2)
-    arrivals = [direct_a1, direct_a2, direct_b, by_x1, by_x2, by_z1, by_z2]
     for k in range(1, chips):
-        near = [arrival[k - 1] for arrival in arrivals]
-        other_far = project(act_far, near, places)
+        chunks = [arrival[k - 1] for arrival in (direct_a, direct_b, by_x, by_z)]
+        source = (mine // 2 - k) % chips * 2 + mine % 2
+        other_far, out = project(act_far, act, chunks, places, source, columns, out)
         received.append(to_sibling(other_far))
-        pieces.append(project(act, near, places))
-        shards.append((mine // 2 - k) % chips * 2 + mine % 2)
-    return collect(pieces + received, shards + [shard ^ 1 for shard in shards])
+        shards.append(source ^ 1)
+    return collect(received, shards, out)
 
 
 def solution(mesh):

time: 53.3 us -> 46.9 us (0.88)
  the two profiles are of different devices: /device:TPU:25 before, /device:TPU:0 now
where the time goes in v2:
time: 46.9 us; the launch traced here: 46.6 us
  Pallas kernels  24.6 us (52%)
  starting transfers between devices  11.8 us (25%)
  waiting for transfers between devices  9.81 us (21%)
    pallas_call x2, Pallas kernels, project(): pl.pallas_call(functools.partial(project_body, len(chunks)), grid_spec=pl...  7.73 us
    ppermute x3, starting transfers between devices, to_near(): return lax.ppermute(x, 'sp', [(i, i ^ bit) for i in range(sp)])  7.42 us
    pallas_call x1, Pallas kernels, activated_inner(): pl.pallas_call(functools.partial(inner_body, tiles), out_shape=jax.ShapeD...  6.82 us
    pallas_call x1, Pallas kernels, gated(): pl.pallas_call(glu_body, grid=(channels // block,), in_specs=[TABLE] + [p...  4.71 us
    ppermute x3, waiting for transfers between devices, to_near(): return lax.ppermute(x, 'sp', [(i, i ^ bit) for i in range(sp)])  4.13 us
    ppermute x1, waiting for transfers between devices, per_device(): direct_b = [lax.ppermute(second, 'dp', perm) for perm in hops]  4.01 us
    ppermute x1, starting transfers between devices, per_device(): direct_a = [lax.ppermute(first, 'dp', perm) for perm in hops]  3.06 us
    pallas_call x1, Pallas kernels, cut(): pl.pallas_call(cut_body, in_specs=[TABLE, STAY], out_specs=[WHOLE] * len(...  2.55 us
  transfers between devices with their start and end apart: 9, of which 4 were waited for; matrix products, arithmetic and copies ran while one was open for 1% of the time, Pallas kernels for 41%

profile of v2, /device:TPU:0, one launch (start us, length us, event | category | flops | bytes accessed | tf_op | source)
XLA Modules:
  0.0 46.6 jit_solution(5019974433276121254)
XLA Ops:
  0.0 0.1 pad_add_fusion.2.place_ref
  0.1 2.5 %cut.1 = (bf16[512,512]{1,0:T(8,128)(2,1)S(1)}, bf16[512,512]{1,0:T(8,128)(2,1)}) custom-call(s32[2]{0:T(128)S(1)} %pad_add_fusion.2.place_ref, bf16[2048,512]{1,0:T(8,128)(2,1)} %refs_0_.1), custom_call_target="tpu_custom_call" | custom-call | tf_op jit(solution)/shard_map/cut/pallas_call | solution.py:201
  2.6 3.1 %collective-permute-start.2 = (bf16[512,512]{1,0:T(8,128)(2,1)S(1)}, bf16[512,512]{1,0:T(8,128)(2,1)S(1)}, u32[]{:S(2)}, u32[]{:S(2)}) collective-permute-start(bf16[512,512]{1,0:T(8,128)(2,1)S(1)} %get-tuple-element.21), channel_id=1, source_target_pairs={{0,2},{1,3},{2,0},{3,1},{4,6},{5,7},{6,4},{7,5},{8,10},{9,11},{10,... | collective-permute-start | bytes 1572872 | tf_op jit(solution)/shard_map/ppermute | solution.py:312
  5.7 4.7 %glu.1 = (bf16[256,2048]{1,0:T(8,128)(2,1)S(1)}, bf16[16,2048]{1,0:T(8,128)(2,1)S(1)}, bf16[16,2048]{1,0:T(8,128)(2,1)S(1)}) custom-call(s32[1]{0:T(128)} %bitcast.4.parity_ref, bf16[2048,256]{1,0:T(8,128)(2,1)} %lin_ref.1, bf16[2048,256]{1,0:T(8,128)(2,1)} %gate_ref.1), custom_call_target="tpu_custom_call" | custom-call | flops 10485760 | bytes 3145728 | tf_op jit(solution)/shard_map/glu/pallas_call | solution.py:45
  10.4 1.6 %collective-permute-start = (bf16[16,2048]{1,0:T(8,128)(2,1)S(1)}, bf16[16,2048]{1,0:T(8,128)(2,1)S(1)}, u32[]{:S(2)}, u32[]{:S(2)}) collective-permute-start(bf16[16,2048]{1,0:T(8,128)(2,1)S(1)} %get-tuple-element.19), channel_id=1, source_target_pairs={{0,4},{4,0},{8,12},{12,8},{16,20},{20,16},{24,28},{28,24},{1,5},{5... | collective-permute-start | bytes 196616 | tf_op jit(solution)/shard_map/ppermute | solution.py:305
  12.0 0.7 %collective-permute-start.1 = (bf16[16,2048]{1,0:T(8,128)(2,1)S(1)}, bf16[16,2048]{1,0:T(8,128)(2,1)S(1)}, u32[]{:S(2)}, u32[]{:S(2)}) collective-permute-start(bf16[16,2048]{1,0:T(8,128)(2,1)S(1)} %get-tuple-element.20), channel_id=1, source_target_pairs={{4,8},{12,16},{20,24},{8,4},{16,12},{24,20},{5,9},{13,17},{21,25},... | collective-permute-start | bytes 196616 | tf_op jit(solution)/shard_map/ppermute | solution.py:318
  12.7 6.8 %conv_inner.1._ = bf16[256,2048]{1,0:T(8,128)(2,1)S(1)} custom-call(bf16[256,2048]{1,0:T(8,128)(2,1)S(1)} %get-tuple-element.22.glu_ref, f32[31,2048]{1,0:T(8,128)S(1)} %copy-done, f32[1,2048]{1,0:T(1,128)S(1)} %bitcast.11, f32[1,2048]{1,0:T(1,128)S(1)} %bitcast.13), custom_call_target="tpu_custom_call" | custom-call | flops 41943040 | bytes 2097152 | tf_op jit(solution)/shard_map/conv_inner/pallas_call | solution.py:142
  19.5 0.0 collective-permute-done.near_ref
  19.5 0.0 collective-permute-done.1.next_ref
  19.5 1.4 %conv_outer.1.near_ref = bf16[256,2048]{1,0:T(8,128)(2,1)S(1)} custom-call(s32[1]{0:T(128)} %bitcast.4.parity_ref, bf16[16,2048]{1,0:T(8,128)(2,1)S(1)} %collective-permute-done.near_ref, bf16[16,2048]{1,0:T(8,128)(2,1)S(1)} %collective-permute-done.1.next_ref, bf16[256,2048]{1,0:T(8,128)(2,1)S(1)} %get-tuple-element.22.glu_ref, ...), custom_call_target="tpu_custom_call", output_to_operand_aliasing={{}: (7, {})} | custom-call | flops 5242880 | bytes 262144 | tf_op jit(solution)/shard_map/conv_outer/pallas_call | solution.py:161
  21.0 0.1 collective-permute-start.3
  21.0 0.6 %collective-permute-start.5 = (bf16[512,512]{1,0:T(8,128)(2,1)}, bf16[512,512]{1,0:T(8,128)(2,1)S(1)}, u32[]{:S(2)}, u32[]{:S(2)}) collective-permute-start(bf16[512,512]{1,0:T(8,128)(2,1)} %get-tuple-element.29), channel_id=1, source_target_pairs={{0,2},{1,3},{2,0},{3,1},{4,6},{5,7},{6,4},{7,5},{8,10},{9,11},{10,... | collective-permute-start | bytes 1572872 | tf_op jit(solution)/shard_map/ppermute | solution.py:313
  21.6 4.3 %collective-permute-start.6 = (bf16[512,512]{1,0:T(8,128)(2,1)S(1)}, bf16[512,512]{1,0:T(8,128)(2,1)}, u32[]{:S(2)}, u32[]{:S(2)}) collective-permute-start(bf16[512,512]{1,0:T(8,128)(2,1)S(1)} %collective-permute-done.2.refs_0_), channel_id=1, source_target_pairs={{0,4},{4,0},{8,12},{12,8},{16,20},{20,16},{24,28},{28,24},{1,5},{5... | collective-permute-start | bytes 1572872 | tf_op jit(solution)/shard_map/ppermute | solution.py:305
  25.9 1.6 %collective-permute-start.7 = (bf16[512,512]{1,0:T(8,128)(2,1)S(1)}, bf16[512,512]{1,0:T(8,128)(2,1)}, u32[]{:S(2)}, u32[]{:S(2)}) collective-permute-start(bf16[512,512]{1,0:T(8,128)(2,1)S(1)} %collective-permute-done.2.refs_0_), channel_id=1, source_target_pairs={{0,8},{4,12},{8,0},{12,4},{16,24},{20,28},{24,16},{28,20},{1,9},{5... | collective-permute-start | bytes 1572872 | tf_op jit(solution)/shard_map/ppermute | solution.py:305
  27.5 0.1 stack.50.place_ref
  27.5 0.1 pad_add_fusion.1.place_ref
  27.6 3.9 %project.2 = (bf16[256,512]{1,0:T(8,128)(2,1)}, bf16[256,2048]{1,0:T(8,128)(2,1)}) custom-call(s32[2]{0:T(128)S(1)} %pad_add_fusion.1.place_ref, bf16[256,2048]{1,0:T(8,128)(2,1)S(1)} %collective-permute-done.3.far_ref, bf16[256,2048]{1,0:T(8,128)(2,1)S(1)} %conv_outer.1.near_ref, bf16[2048,512]{1,0:T(8,128)(2,1)} %refs_0_.1), custom_call_target="tpu_custom_call" | custom-call | flops 1073741824 | bytes 4194304 | tf_op jit(solution)/shard_map/project/pallas_call | solution.py:241
  31.6 4.0 %collective-permute-done.5.refs_1_ = bf16[512,512]{1,0:T(8,128)(2,1)S(1)} collective-permute-done((bf16[512,512]{1,0:T(8,128)(2,1)}, bf16[512,512]{1,0:T(8,128)(2,1)S(1)}, u32[]{:S(2)}, u32[]{:S(2)}) %collective-permute-start.5) | collective-permute-done | bytes 524320 | tf_op jit(solution)/shard_map/ppermute | solution.py:313
  35.6 2.7 %collective-permute-done.6.refs_2_ = bf16[512,512]{1,0:T(8,128)(2,1)} collective-permute-done((bf16[512,512]{1,0:T(8,128)(2,1)S(1)}, bf16[512,512]{1,0:T(8,128)(2,1)}, u32[]{:S(2)}, u32[]{:S(2)}) %collective-permute-start.6) | collective-permute-done | bytes 524320 | tf_op jit(solution)/shard_map/ppermute | solution.py:305
  38.2 1.5 %collective-permute-done.7.refs_3_ = bf16[512,512]{1,0:T(8,128)(2,1)} collective-permute-done((bf16[512,512]{1,0:T(8,128)(2,1)S(1)}, bf16[512,512]{1,0:T(8,128)(2,1)}, u32[]{:S(2)}, u32[]{:S(2)}) %collective-permute-start.7) | collective-permute-done | bytes 524320 | tf_op jit(solution)/shard_map/ppermute | solution.py:305
  39.7 3.8 %project.3 = (bf16[256,512]{1,0:T(8,128)(2,1)}, bf16[256,2048]{1,0:T(8,128)(2,1)}) custom-call(s32[5]{0:T(128)S(1)} %stack.50.place_ref, bf16[256,2048]{1,0:T(8,128)(2,1)S(1)} %collective-permute-done.3.far_ref, bf16[256,2048]{1,0:T(8,128)(2,1)S(1)} %conv_outer.1.near_ref, ...), custom_call_target="tpu_custom_call", output_to_operand_aliasing={{1}: (7, {})} | custom-call | flops 1073741824 | bytes 4194304 | tf_op jit(solution)/shard_map/project/pallas_call | solution.py:241
  43.5 0.1 pad_add_fusion.place_ref
  43.6 1.7 %collective-permute-done.8.refs_1_ = bf16[256,512]{1,0:T(8,128)(2,1)S(1)} collective-permute-done((bf16[256,512]{1,0:T(8,128)(2,1)}, bf16[256,512]{1,0:T(8,128)(2,1)S(1)}, u32[]{:S(2)}, u32[]{:S(2)}) %collective-permute-start.8) | collective-permute-done | bytes 262176 | tf_op jit(solution)/shard_map/ppermute | solution.py:302
  45.2 1.3 %collect.1 = bf16[256,2048]{1,0:T(8,128)(2,1)} custom-call(s32[2]{0:T(128)S(1)} %pad_add_fusion.place_ref, bf16[256,512]{1,0:T(8,128)(2,1)S(1)} %collective-permute-done.4.refs_0_, bf16[256,512]{1,0:T(8,128)(2,1)S(1)} %collective-permute-done.8.refs_1_, bf16[256,2048]{1,0:T(8,128)(2,1)} %get-tuple-element.32.refs_2_), custom_call_target="tpu_custom_call", output_to_operand_aliasing={{}: (3, {})} | custom-call | tf_op jit(solution)/shard_map/collect/pallas_call | solution.py:281
  (11 shorter events, 0.0 us)
Async XLA Ops:
  0.1 12.6 %copy-start = (f32[31,2048]{1,0:T(8,128)S(1)}, f32[31,2048]{1,0:T(8,128)}, u32[]{:S(2)}) copy-start(f32[31,2048]{1,0:T(8,128)} %w_ref.5) | copy-start | bytes 761860
  0.1 12.6 %copy-start.1 = (f32[2048]{0:T(1024)S(1)}, f32[2048]{0:T(1024)}, u32[]{:S(2)}) copy-start(f32[2048]{0:T(1024)} %param.9) | copy-start | bytes 24580
  0.1 12.6 %copy-start.2 = (f32[2048]{0:T(1024)S(1)}, f32[2048]{0:T(1024)}, u32[]{:S(2)}) copy-start(f32[2048]{0:T(1024)} %param.10) | copy-start | bytes 24580
  2.6 16.9 %collective-permute-start.2 = (bf16[512,512]{1,0:T(8,128)(2,1)S(1)}, bf16[512,512]{1,0:T(8,128)(2,1)S(1)}, u32[]{:S(2)}, u32[]{:S(2)}) collective-permute-start(bf16[512,512]{1,0:T(8,128)(2,1)S(1)} %get-tuple-element.21), channel_id=1, source_target_pairs={{0,2},{1,3},{2,0},{3,1},{4,6},{5,7},{6,4},{7,5},{8,10},{9,11},{10,... | collective-permute-start | bytes 1572872 | tf_op jit(solution)/shard_map/ppermute | solution.py:312
  10.4 9.1 %collective-permute-start = (bf16[16,2048]{1,0:T(8,128)(2,1)S(1)}, bf16[16,2048]{1,0:T(8,128)(2,1)S(1)}, u32[]{:S(2)}, u32[]{:S(2)}) collective-permute-start(bf16[16,2048]{1,0:T(8,128)(2,1)S(1)} %get-tuple-element.19), channel_id=1, source_target_pairs={{0,4},{4,0},{8,12},{12,8},{16,20},{20,16},{24,28},{28,24},{1,5},{5... | collective-permute-start | bytes 196616 | tf_op jit(solution)/shard_map/ppermute | solution.py:305
  12.0 7.5 %collective-permute-start.1 = (bf16[16,2048]{1,0:T(8,128)(2,1)S(1)}, bf16[16,2048]{1,0:T(8,128)(2,1)S(1)}, u32[]{:S(2)}, u32[]{:S(2)}) collective-permute-start(bf16[16,2048]{1,0:T(8,128)(2,1)S(1)} %get-tuple-element.20), channel_id=1, source_target_pairs={{4,8},{12,16},{20,24},{8,4},{16,12},{24,20},{5,9},{13,17},{21,25},... | collective-permute-start | bytes 196616 | tf_op jit(solution)/shard_map/ppermute | solution.py:318
  21.0 6.7 %collective-permute-start.3 = (bf16[256,2048]{1,0:T(8,128)(2,1)S(1)}, bf16[256,2048]{1,0:T(8,128)(2,1)S(1)}, u32[]{:S(2)}, u32[]{:S(2)}) collective-permute-start(bf16[256,2048]{1,0:T(8,128)(2,1)S(1)} %conv_outer.1.near_ref), channel_id=1, source_target_pairs={{0,1},{1,0},{2,3},{3,2},{4,5},{5,4},{6,7},{7,6},{8,9},{9,8},{10,11... | collective-permute-start | bytes 3145736 | tf_op jit(solution)/shard_map/ppermute | solution.py:302
  21.0 14.5 %collective-permute-start.5 = (bf16[512,512]{1,0:T(8,128)(2,1)}, bf16[512,512]{1,0:T(8,128)(2,1)S(1)}, u32[]{:S(2)}, u32[]{:S(2)}) collective-permute-start(bf16[512,512]{1,0:T(8,128)(2,1)} %get-tuple-element.29), channel_id=1, source_target_pairs={{0,2},{1,3},{2,0},{3,1},{4,6},{5,7},{6,4},{7,5},{8,10},{9,11},{10,... | collective-permute-start | bytes 1572872 | tf_op jit(solution)/shard_map/ppermute | solution.py:313
  21.6 16.6 %collective-permute-start.6 = (bf16[512,512]{1,0:T(8,128)(2,1)S(1)}, bf16[512,512]{1,0:T(8,128)(2,1)}, u32[]{:S(2)}, u32[]{:S(2)}) collective-permute-start(bf16[512,512]{1,0:T(8,128)(2,1)S(1)} %collective-permute-done.2.refs_0_), channel_id=1, source_target_pairs={{0,4},{4,0},{8,12},{12,8},{16,20},{20,16},{24,28},{28,24},{1,5},{5... | collective-permute-start | bytes 1572872 | tf_op jit(solution)/shard_map/ppermute | solution.py:305
  25.9 13.8 %collective-permute-start.7 = (bf16[512,512]{1,0:T(8,128)(2,1)S(1)}, bf16[512,512]{1,0:T(8,128)(2,1)}, u32[]{:S(2)}, u32[]{:S(2)}) collective-permute-start(bf16[512,512]{1,0:T(8,128)(2,1)S(1)} %collective-permute-done.2.refs_0_), channel_id=1, source_target_pairs={{0,8},{4,12},{8,0},{12,4},{16,24},{20,28},{24,16},{28,20},{1,9},{5... | collective-permute-start | bytes 1572872 | tf_op jit(solution)/shard_map/ppermute | solution.py:305
  31.6 12.0 %collective-permute-start.4 = (bf16[256,512]{1,0:T(8,128)(2,1)}, bf16[256,512]{1,0:T(8,128)(2,1)S(1)}, u32[]{:S(2)}, u32[]{:S(2)}) collective-permute-start(bf16[256,512]{1,0:T(8,128)(2,1)} %get-tuple-element.27), channel_id=1, source_target_pairs={{0,1},{1,0},{2,3},{3,2},{4,5},{5,4},{6,7},{7,6},{8,9},{9,8},{10,11... | collective-permute-start | bytes 786440 | tf_op jit(solution)/shard_map/ppermute | solution.py:302
  43.5 1.7 %collective-permute-start.8 = (bf16[256,512]{1,0:T(8,128)(2,1)}, bf16[256,512]{1,0:T(8,128)(2,1)S(1)}, u32[]{:S(2)}, u32[]{:S(2)}) collective-permute-start(bf16[256,512]{1,0:T(8,128)(2,1)} %get-tuple-element.31), channel_id=1, source_target_pairs={{0,1},{1,0},{2,3},{3,2},{4,5},{5,4},{6,7},{7,6},{8,9},{9,8},{10,11... | collective-permute-start | bytes 786440 | tf_op jit(solution)/shard_map/ppermute | solution.py:302

commit v3 on v0

--- a/solution.py
+++ b/solution.py
@@ -11,6 +11,9 @@
 LANES = 128
 EDGE = 16
 EPS = 1e-05
+WHOLE = pl.BlockSpec(memory_space=pltpu.VMEM)
+STAY = pl.BlockSpec(memory_space=pltpu.HBM)
+TABLE = pl.BlockSpec(memory_space=pltpu.SMEM)
 
 
 def params(semantics=None):
@@ -21,22 +24,24 @@
     return pl.CostEstimate(flops=flops, transcendentals=0, bytes_accessed=nbytes)
 
 
-def glu_body(lin_ref, gate_ref, out_ref, head_ref, tail_ref):
+def glu_body(parity_ref, lin_ref, gate_ref, out_ref, near_ref, next_ref):
     gate = gate_ref[...].astype(jnp.float32)
     glu = (lin_ref[...].astype(jnp.float32) * jax.nn.sigmoid(gate)).T.astype(jnp.bfloat16)
     out_ref[...] = glu
-    head_ref[...] = glu[:EDGE]
-    tail_ref[...] = glu[glu.shape[0] - EDGE :]
-
-
-def gated(lin_pre, gate_pre):
+    head, tail = glu[:EDGE], glu[glu.shape[0] - EDGE :]
+    even = parity_ref[0] == 0
+    near_ref[...] = jnp.where(even, tail, head)
+    next_ref[...] = jnp.where(even, head, tail)
+
+
+def gated(parity, lin_pre, gate_pre):
     channels, tokens = lin_pre.shape
     block = 256
     edge = pl.BlockSpec((EDGE, block), lambda i: (0, i))
     return pl.pallas_call(
         glu_body,
         grid=(channels // block,),
-        in_specs=[pl.BlockSpec((block, tokens), lambda i: (i, 0))] * 2,
+        in_specs=[TABLE] + [pl.BlockSpec((block, tokens), lambda i: (i, 0))] * 2,
         out_specs=[pl.BlockSpec((tokens, block), lambda i: (0, i)), edge, edge],
         out_shape=[
             jax.ShapeDtypeStruct((tokens, channels), jnp.bfloat16),
@@ -46,7 +51,7 @@
         compiler_params=params(("arbitrary",)),
         cost_estimate=cost(20 * channels * tokens, 6 * channels * tokens),
         name="glu",
-    )(lin_pre, gate_pre)
+    )(parity, lin_pre, gate_pre)
 
 
 def conv_norm(cells, w_ref, gain_ref, shift_ref, mixed, start, tiles, store):
@@ -106,13 +111,14 @@
     lax.fori_loop(0, (glu_ref.shape[0] - 2 * EDGE) // span, chunk, 0)
 
 
-def outer_body(before_ref, after_ref, glu_ref, w_ref, gain_ref, shift_ref, _, out_ref, cells, mixed):
+def outer_body(parity_ref, near_ref, next_ref, glu_ref, w_ref, gain_ref, shift_ref, _, out_ref, cells, mixed):
     side = pl.program_id(0)
     blocks = cells.shape[0]
     for block in range(blocks):
         lanes = pl.ds(block * LANES, LANES)
         own = glu_ref[:, lanes].astype(jnp.float32)
-        halo = jnp.where(side == 0, before_ref[:, lanes], after_ref[:, lanes]).astype(jnp.float32)
+        halo = jnp.where(side != parity_ref[0], near_ref[:, lanes], next_ref[:, lanes])
+        halo = halo.astype(jnp.float32)
         cells[block, pl.ds(EDGE, 2 * EDGE), :] = jnp.where(side == 0, own, 0.0)
         cells[block, pl.ds(0, EDGE), :] = jnp.where(side == 0, halo, own[:EDGE])
         cells[block, pl.ds(EDGE, EDGE), :] = jnp.where(side == 0, own[:EDGE], own[EDGE:])
@@ -142,7 +148,7 @@
     )(glu, w_depth, gain, shift)
 
 
-def activated_outer(before, after, glu, w_depth, gain, shift, act):
+def activated_outer(parity, near, ahead, glu, w_depth, gain, shift, act):
     tokens, channels = glu.shape
     blocks = channels // LANES
     whole = pl.BlockSpec((EDGE, channels), lambda i: (0, 0))
@@ -152,6 +158,7 @@
         outer_body,
         grid=(2,),
         in_specs=[
+            TABLE,
             whole,
             whole,
             pl.BlockSpec((2 * EDGE, channels), lambda i: (i * (tokens // (2 * EDGE) - 1), 0)),
@@ -166,16 +173,11 @@
             pltpu.VMEM((blocks, 3 * EDGE, LANES), jnp.float32),
             pltpu.VMEM((blocks, EDGE, LANES), jnp.float32),
         ],
-        input_output_aliases={6: 0},
+        input_output_aliases={7: 0},
         compiler_params=params(("arbitrary",)),
         cost_estimate=cost(80 * channels * 2 * EDGE, 8 * channels * EDGE),
         name="conv_outer",
-    )(before, after, glu, w_depth, gain, shift, act)
-
-
-WHOLE = pl.BlockSpec(memory_space=pltpu.VMEM)
-STAY = pl.BlockSpec(memory_space=pltpu.HBM)
-TABLE = pl.BlockSpec(memory_space=pltpu.SMEM)
+    )(parity, near, ahead, glu, w_depth, gain, shift, act)
 
 
 def quarters_body(place_ref, w_ref, *refs):
@@ -263,6 +265,7 @@
     chips = dp // 2
     mine = lax.axis_index("dp")
     spot = lax.axis_index("sp") % 4
+    parity = (lax.axis_index("sp") % 2)[None]
 
     def to_sibling(x):
         return lax.ppermute(x, "dp", [(i, i ^ 1) for i in range(dp)])
@@ -270,24 +273,25 @@
     def to_near(x, bit):
         return lax.ppermute(x, "sp", [(i, i ^ bit) for i in range(sp)])
 
-    first, second = quarters(w_out, (spot, 3 - spot))
+    (first,) = quarters(w_out, (spot,))
+    (second,) = quarters(w_out, (3 - spot,))
     hops = [
         [(i, (i // 2 + k) % chips * 2 + i % 2) for i in range(dp)] for k in range(1, chips)
     ]
     direct_a = [lax.ppermute(first, "dp", perm) for perm in hops]
     direct_b = [lax.ppermute(second, "dp", perm) for perm in hops]
 
-    glu, head, tail = gated(lin_pre, gate_pre)
-    ends = sp - 1
-    before = lax.ppermute(tail, "sp", [(i, i + 1) for i in range(ends)])
-    after = lax.ppermute(head, "sp", [(i + 1, i) for i in range(ends)])
+    glu, to_pair, to_next = gated(parity, lin_pre, gate_pre)
+    odd = [(i, i + 1) for i in range(1, sp - 1, 2)]
+    from_pair = to_near(to_pair, 1)
+    from_next = lax.ppermute(to_next, "sp", odd + [(j, i) for i, j in odd])
     gain, shift = ln_gain[None, :], ln_shift[None, :]
     act = activated_inner(glu, w_depth, gain, shift)
     direct_a, act = lax.optimization_barrier((direct_a, act))
     by_x = [to_near(a, 1) for a in direct_a]
     by_z = [to_near(a, 2) for a in direct_a]
-    before, after, act = lax.optimization_barrier((before, after, act))
-    act = activated_outer(before, after, glu, w_depth, gain, shift, act)
+    from_pair, from_next, act = lax.optimization_barrier((from_pair, from_next, act))
+    act = activated_outer(parity, from_pair, from_next, glu, w_depth, gain, shift, act)
 
     act_far = to_sibling(act)
     pieces, shards = [project(act, [w_out], (spot,))], [mine]

time: 49.3 us -> 49.1 us (level)
  starting transfers between devices: 13.1 us -> 10.7 us
  Pallas kernels: 22.8 us -> 24.2 us
  waiting for transfers between devices: 12.6 us -> 13.6 us
    ppermute x2 -> x1, starting transfers between devices: 4.69 us -> 0.65 us  [per_device(): from_next = lax.ppermute(to_next, 'sp', odd + [(j, i) for i, j in odd])]
    ppermute x1, waiting for transfers between devices: 0.01 us -> 1.97 us  [per_device(): direct_a = [lax.ppermute(first, 'dp', perm) for perm in hops]]
    pallas_call x1 -> x2, Pallas kernels: 2.66 us -> 3.97 us  [quarters(): pl.pallas_call(quarters_body, in_specs=[TABLE, STAY], out_specs=[WHOLE] *...]
    ppermute x2 -> x3, starting transfers between devices: 3.76 us -> 4.62 us  [to_near(): return lax.ppermute(x, 'sp', [(i, i ^ bit) for i in range(sp)])]
    ppermute x2 -> x3, waiting for transfers between devices: 3.57 us -> 2.76 us  [to_near(): return lax.ppermute(x, 'sp', [(i, i ^ bit) for i in range(sp)])]
    ppermute x1, starting transfers between devices: 1.04 us -> 1.8 us  [per_device(): direct_b = [lax.ppermute(second, 'dp', perm) for perm in hops]]
  transfers between devices with their start and end apart: 9 -> 9, of which waited for: 3 -> 4; matrix products, arithmetic and copies ran while one was open for 0% -> 0% of each run, Pallas kernels for 28% -> 32%
where the time goes in v3:
time: 49.1 us; the launch traced here: 48.9 us
  Pallas kernels  24.2 us (49%)
  waiting for transfers between devices  13.6 us (28%)
  starting transfers between devices  10.7 us (22%)
    ppermute x1, waiting for transfers between devices, per_device(): direct_b = [lax.ppermute(second, 'dp', perm) for perm in hops]  8.91 us
    pallas_call x4, Pallas kernels, project(): pl.pallas_call(project_body, in_specs=[TABLE] + [WHOLE] * (1 + len(chunks...  8.82 us
    pallas_call x1, Pallas kernels, activated_inner(): pl.pallas_call(functools.partial(inner_body, tiles), out_shape=jax.ShapeD...  6.82 us
    ppermute x3, starting transfers between devices, to_near(): return lax.ppermute(x, 'sp', [(i, i ^ bit) for i in range(sp)])  4.62 us
    pallas_call x2, Pallas kernels, quarters(): pl.pallas_call(quarters_body, in_specs=[TABLE, STAY], out_specs=[WHOLE] *...  3.97 us
    ppermute x1, starting transfers between devices, per_device(): direct_a = [lax.ppermute(first, 'dp', perm) for perm in hops]  3.08 us
    ppermute x3, waiting for transfers between devices, to_near(): return lax.ppermute(x, 'sp', [(i, i ^ bit) for i in range(sp)])  2.76 us
    ppermute x1, waiting for transfers between devices, per_device(): direct_a = [lax.ppermute(first, 'dp', perm) for perm in hops]  1.97 us
  transfers between devices with their start and end apart: 9, of which 4 were waited for; matrix products, arithmetic and copies ran while one was open for 0% of the time, Pallas kernels for 32%

profile of v3, /device:TPU:0, one launch (start us, length us, event | category | flops | bytes accessed | tf_op | source)
XLA Modules:
  0.0 48.9 jit_solution(12630332284017800028)
XLA Ops:
  0.0 2.0 %quarters.2 = bf16[512,512]{1,0:T(8,128)(2,1)} custom-call(s32[1]{0:T(128)} %bitcast.4.place_ref, bf16[2048,512]{1,0:T(8,128)(2,1)} %refs_0_.3), custom_call_target="tpu_custom_call" | custom-call | tf_op jit(solution)/shard_map/quarters/pallas_call | solution.py:198
  2.0 3.1 %collective-permute-start = (bf16[512,512]{1,0:T(8,128)(2,1)}, bf16[512,512]{1,0:T(8,128)(2,1)}, u32[]{:S(2)}, u32[]{:S(2)}) collective-permute-start(bf16[512,512]{1,0:T(8,128)(2,1)} %quarters.2), channel_id=1, source_target_pairs={{0,2},{1,3},{2,0},{3,1},{4,6},{5,7},{6,4},{7,5},{8,10},{9,11},{10,... | collective-permute-start | bytes 1572872 | tf_op jit(solution)/shard_map/ppermute | solution.py:281
  5.1 1.2 %glu.1 = (bf16[256,2048]{1,0:T(8,128)(2,1)S(1)}, bf16[16,2048]{1,0:T(8,128)(2,1)S(1)}, bf16[16,2048]{1,0:T(8,128)(2,1)S(1)}) custom-call(s32[1]{0:T(128)} %bitcast.5.parity_ref, bf16[2048,256]{1,0:T(8,128)(2,1)S(1)} %copy-done.1, bf16[2048,256]{1,0:T(8,128)(2,1)S(1)} %copy-done.2), custom_call_target="tpu_custom_call" | custom-call | flops 10485760 | bytes 3145728 | tf_op jit(solution)/shard_map/glu/pallas_call | solution.py:41
  6.3 1.6 %collective-permute-start.4 = (bf16[16,2048]{1,0:T(8,128)(2,1)S(1)}, bf16[16,2048]{1,0:T(8,128)(2,1)S(1)}, u32[]{:S(2)}, u32[]{:S(2)}) collective-permute-start(bf16[16,2048]{1,0:T(8,128)(2,1)S(1)} %get-tuple-element.21), channel_id=1, source_target_pairs={{0,4},{4,0},{8,12},{12,8},{16,20},{20,16},{24,28},{28,24},{1,5},{5... | collective-permute-start | bytes 196616 | tf_op jit(solution)/shard_map/ppermute | solution.py:274
  7.8 0.7 %collective-permute-start.5 = (bf16[16,2048]{1,0:T(8,128)(2,1)S(1)}, bf16[16,2048]{1,0:T(8,128)(2,1)S(1)}, u32[]{:S(2)}, u32[]{:S(2)}) collective-permute-start(bf16[16,2048]{1,0:T(8,128)(2,1)S(1)} %get-tuple-element.22), channel_id=1, source_target_pairs={{4,8},{12,16},{20,24},{8,4},{16,12},{24,20},{5,9},{13,17},{21,25},... | collective-permute-start | bytes 196616 | tf_op jit(solution)/shard_map/ppermute | solution.py:287
  8.5 6.8 %conv_inner.1._ = bf16[256,2048]{1,0:T(8,128)(2,1)S(1)} custom-call(bf16[256,2048]{1,0:T(8,128)(2,1)S(1)} %get-tuple-element.19.glu_ref, f32[31,2048]{1,0:T(8,128)S(1)} %copy-done.3, f32[1,2048]{1,0:T(1,128)S(1)} %bitcast.11, f32[1,2048]{1,0:T(1,128)S(1)} %bitcast.13), custom_call_target="tpu_custom_call" | custom-call | flops 41943040 | bytes 2097152 | tf_op jit(solution)/shard_map/conv_inner/pallas_call | solution.py:138
  15.4 2.0 %collective-permute-done.refs_0_ = bf16[512,512]{1,0:T(8,128)(2,1)} collective-permute-done((bf16[512,512]{1,0:T(8,128)(2,1)}, bf16[512,512]{1,0:T(8,128)(2,1)}, u32[]{:S(2)}, u32[]{:S(2)}) %collective-permute-start) | collective-permute-done | bytes 524320 | tf_op jit(solution)/shard_map/ppermute | solution.py:281
  17.3 1.4 %conv_outer.1.act_ref = bf16[256,2048]{1,0:T(8,128)(2,1)S(1)} custom-call(s32[1]{0:T(128)} %bitcast.5.parity_ref, bf16[16,2048]{1,0:T(8,128)(2,1)S(1)} %collective-permute-done.4.near_ref, bf16[16,2048]{1,0:T(8,128)(2,1)S(1)} %collective-permute-done.5.next_ref, bf16[256,2048]{1,0:T(8,128)(2,1)S(1)} %get-tuple-element.19.glu_ref, ...), custom_call_target="tpu_custom_call", output_to_operand_aliasing={{}: (7, {})} | custom-call | flops 5242880 | bytes 262144 | tf_op jit(solution)/shard_map/conv_outer/pallas_call | solution.py:157
  18.8 0.1 collective-permute-start.6
  18.8 2.0 %quarters.3 = bf16[512,512]{1,0:T(8,128)(2,1)} custom-call(s32[1]{0:T(128)} %bitcast.8.place_ref, bf16[2048,512]{1,0:T(8,128)(2,1)} %refs_0_.3), custom_call_target="tpu_custom_call" | custom-call | tf_op jit(solution)/shard_map/quarters/pallas_call | solution.py:198
  20.8 1.8 %collective-permute-start.3 = (bf16[512,512]{1,0:T(8,128)(2,1)}, bf16[512,512]{1,0:T(8,128)(2,1)}, u32[]{:S(2)}, u32[]{:S(2)}) collective-permute-start(bf16[512,512]{1,0:T(8,128)(2,1)} %quarters.3), channel_id=1, source_target_pairs={{0,2},{1,3},{2,0},{3,1},{4,6},{5,7},{6,4},{7,5},{8,10},{9,11},{10,... | collective-permute-start | bytes 1572872 | tf_op jit(solution)/shard_map/ppermute | solution.py:282
  22.6 1.6 %collective-permute-start.2 = (bf16[512,512]{1,0:T(8,128)(2,1)}, bf16[512,512]{1,0:T(8,128)(2,1)}, u32[]{:S(2)}, u32[]{:S(2)}) collective-permute-start(bf16[512,512]{1,0:T(8,128)(2,1)} %collective-permute-done.refs_0_), channel_id=1, source_target_pairs={{0,8},{4,12},{8,0},{12,4},{16,24},{20,28},{24,16},{28,20},{1,9},{5... | collective-permute-start | bytes 1572872 | tf_op jit(solution)/shard_map/ppermute | solution.py:274
  24.2 1.5 %collective-permute-start.1 = (bf16[512,512]{1,0:T(8,128)(2,1)}, bf16[512,512]{1,0:T(8,128)(2,1)}, u32[]{:S(2)}, u32[]{:S(2)}) collective-permute-start(bf16[512,512]{1,0:T(8,128)(2,1)} %collective-permute-done.refs_0_), channel_id=1, source_target_pairs={{0,4},{4,0},{8,12},{12,8},{16,20},{20,16},{24,28},{28,24},{1,5},{5... | collective-permute-start | bytes 1572872 | tf_op jit(solution)/shard_map/ppermute | solution.py:274
  25.7 0.1 pad_add_fusion.1.place_ref
  25.8 0.7 %project.4.refs_0_ = bf16[256,512]{1,0:T(8,128)(2,1)S(1)} custom-call(s32[1]{0:T(128)} %bitcast.4.place_ref, bf16[256,2048]{1,0:T(8,128)(2,1)S(1)} %conv_outer.1.act_ref, bf16[2048,512]{1,0:T(8,128)(2,1)S(1)} %copy-done), custom_call_target="tpu_custom_call" | custom-call | flops 536870912 | bytes 3145728 | tf_op jit(solution)/shard_map/project/pallas_call | solution.py:226
  26.5 8.9 %collective-permute-done.3.refs_1_ = bf16[512,512]{1,0:T(8,128)(2,1)} collective-permute-done((bf16[512,512]{1,0:T(8,128)(2,1)}, bf16[512,512]{1,0:T(8,128)(2,1)}, u32[]{:S(2)}, u32[]{:S(2)}) %collective-permute-start.3) | collective-permute-done | bytes 524320 | tf_op jit(solution)/shard_map/ppermute | solution.py:282
  35.4 1.5 %collective-permute-done.2.refs_3_ = bf16[512,512]{1,0:T(8,128)(2,1)} collective-permute-done((bf16[512,512]{1,0:T(8,128)(2,1)}, bf16[512,512]{1,0:T(8,128)(2,1)}, u32[]{:S(2)}, u32[]{:S(2)}) %collective-permute-start.2) | collective-permute-done | bytes 524320 | tf_op jit(solution)/shard_map/ppermute | solution.py:274
  36.9 1.3 %collective-permute-done.1.refs_2_ = bf16[512,512]{1,0:T(8,128)(2,1)} collective-permute-done((bf16[512,512]{1,0:T(8,128)(2,1)}, bf16[512,512]{1,0:T(8,128)(2,1)}, u32[]{:S(2)}, u32[]{:S(2)}) %collective-permute-start.1) | collective-permute-done | bytes 524320 | tf_op jit(solution)/shard_map/ppermute | solution.py:274
  38.2 3.3 %project.7 = bf16[256,512]{1,0:T(8,128)(2,1)} custom-call(s32[4]{0:T(128)S(1)} %pad_add_fusion.1.place_ref, bf16[256,2048]{1,0:T(8,128)(2,1)} %collective-permute-done.6.act_ref, bf16[512,512]{1,0:T(8,128)(2,1)} %collective-permute-done.refs_0_, bf16[512,512]{1,0:T(8,128)(2,1)} %collective-permute-done.3.refs_1_, ...), custom_call_target="tpu_custom_call" | custom-call | flops 536870912 | bytes 3145728 | tf_op jit(solution)/shard_map/project/pallas_call | solution.py:226
  41.4 2.6 %project.6 = bf16[256,512]{1,0:T(8,128)(2,1)} custom-call(s32[1]{0:T(128)} %bitcast.4.place_ref, bf16[256,2048]{1,0:T(8,128)(2,1)} %collective-permute-done.6.act_ref, bf16[2048,512]{1,0:T(8,128)(2,1)S(1)} %copy-done), custom_call_target="tpu_custom_call" | custom-call | flops 536870912 | bytes 3145728 | tf_op jit(solution)/shard_map/project/pallas_call | solution.py:226
  44.1 0.5 %collective-permute-start.7 = (bf16[256,512]{1,0:T(8,128)(2,1)}, bf16[256,512]{1,0:T(8,128)(2,1)S(1)}, u32[]{:S(2)}, u32[]{:S(2)}) collective-permute-start(bf16[256,512]{1,0:T(8,128)(2,1)} %project.6), channel_id=1, source_target_pairs={{0,1},{1,0},{2,3},{3,2},{4,5},{5,4},{6,7},{7,6},{8,9},{9,8},{10,11... | collective-permute-start | bytes 786440 | tf_op jit(solution)/shard_map/ppermute | solution.py:271
  44.6 0.1 pad_add_fusion.place_ref
  44.6 2.2 %project.5.refs_1_ = bf16[256,512]{1,0:T(8,128)(2,1)S(1)} custom-call(s32[4]{0:T(128)S(1)} %pad_add_fusion.1.place_ref, bf16[256,2048]{1,0:T(8,128)(2,1)S(1)} %conv_outer.1.act_ref, bf16[512,512]{1,0:T(8,128)(2,1)} %collective-permute-done.refs_0_, bf16[512,512]{1,0:T(8,128)(2,1)} %collective-permute-done.3.refs_1_, ...), custom_call_target="tpu_custom_call" | custom-call | flops 536870912 | bytes 3145728 | tf_op jit(solution)/shard_map/project/pallas_call | solution.py:226
  46.9 2.0 %collect.1 = bf16[256,2048]{1,0:T(8,128)(2,1)} custom-call(s32[4]{0:T(128)S(1)} %pad_add_fusion.place_ref, bf16[256,512]{1,0:T(8,128)(2,1)S(1)} %project.4.refs_0_, bf16[256,512]{1,0:T(8,128)(2,1)S(1)} %project.5.refs_1_, bf16[256,512]{1,0:T(8,128)(2,1)S(1)} %collective-permute-done.7.refs_2_, bf16[256,512]{1,0:T(8,128)(2,1)} %collective-permute-done.8.refs_3_), custom_call_target="tpu_custom_call" | custom-call | tf_op jit(solution)/shard_map/collect/pallas_call | solution.py:252
  (18 shorter events, 0.0 us)
Async XLA Ops:
  0.0 5.1 %copy-start.2 = (bf16[2048,256]{1,0:T(8,128)(2,1)S(1)}, bf16[2048,256]{1,0:T(8,128)(2,1)}, u32[]{:S(2)}) copy-start(bf16[2048,256]{1,0:T(8,128)(2,1)} %gate_ref.1) | copy-start | bytes 3145732
  0.0 5.1 %copy-start.1 = (bf16[2048,256]{1,0:T(8,128)(2,1)S(1)}, bf16[2048,256]{1,0:T(8,128)(2,1)}, u32[]{:S(2)}) copy-start(bf16[2048,256]{1,0:T(8,128)(2,1)} %lin_ref.1) | copy-start | bytes 3145732
  0.0 8.5 %copy-start.3 = (f32[31,2048]{1,0:T(8,128)S(1)}, f32[31,2048]{1,0:T(8,128)}, u32[]{:S(2)}) copy-start(f32[31,2048]{1,0:T(8,128)} %w_ref.7) | copy-start | bytes 761860
  0.0 8.5 %copy-start.4 = (f32[2048]{0:T(1024)S(1)}, f32[2048]{0:T(1024)}, u32[]{:S(2)}) copy-start(f32[2048]{0:T(1024)} %param.9) | copy-start | bytes 24580
  0.0 8.5 %copy-start.5 = (f32[2048]{0:T(1024)S(1)}, f32[2048]{0:T(1024)}, u32[]{:S(2)}) copy-start(f32[2048]{0:T(1024)} %param.10) | copy-start | bytes 24580
  2.0 15.3 %collective-permute-start = (bf16[512,512]{1,0:T(8,128)(2,1)}, bf16[512,512]{1,0:T(8,128)(2,1)}, u32[]{:S(2)}, u32[]{:S(2)}) collective-permute-start(bf16[512,512]{1,0:T(8,128)(2,1)} %quarters.2), channel_id=1, source_target_pairs={{0,2},{1,3},{2,0},{3,1},{4,6},{5,7},{6,4},{7,5},{8,10},{9,11},{10,... | collective-permute-start | bytes 1572872 | tf_op jit(solution)/shard_map/ppermute | solution.py:281
  6.3 11.0 %collective-permute-start.4 = (bf16[16,2048]{1,0:T(8,128)(2,1)S(1)}, bf16[16,2048]{1,0:T(8,128)(2,1)S(1)}, u32[]{:S(2)}, u32[]{:S(2)}) collective-permute-start(bf16[16,2048]{1,0:T(8,128)(2,1)S(1)} %get-tuple-element.21), channel_id=1, source_target_pairs={{0,4},{4,0},{8,12},{12,8},{16,20},{20,16},{24,28},{28,24},{1,5},{5... | collective-permute-start | bytes 196616 | tf_op jit(solution)/shard_map/ppermute | solution.py:274
  7.8 9.5 %collective-permute-start.5 = (bf16[16,2048]{1,0:T(8,128)(2,1)S(1)}, bf16[16,2048]{1,0:T(8,128)(2,1)S(1)}, u32[]{:S(2)}, u32[]{:S(2)}) collective-permute-start(bf16[16,2048]{1,0:T(8,128)(2,1)S(1)} %get-tuple-element.22), channel_id=1, source_target_pairs={{4,8},{12,16},{20,24},{8,4},{16,12},{24,20},{5,9},{13,17},{21,25},... | collective-permute-start | bytes 196616 | tf_op jit(solution)/shard_map/ppermute | solution.py:287
  18.8 7.0 %copy-start = (bf16[2048,512]{1,0:T(8,128)(2,1)S(1)}, bf16[2048,512]{1,0:T(8,128)(2,1)}, u32[]{:S(2)}) copy-start(bf16[2048,512]{1,0:T(8,128)(2,1)} %refs_0_.3) | copy-start | bytes 6291460
  18.8 19.4 %collective-permute-start.6 = (bf16[256,2048]{1,0:T(8,128)(2,1)S(1)}, bf16[256,2048]{1,0:T(8,128)(2,1)}, u32[]{:S(2)}, u32[]{:S(2)}) collective-permute-start(bf16[256,2048]{1,0:T(8,128)(2,1)S(1)} %conv_outer.1.act_ref), channel_id=1, source_target_pairs={{0,1},{1,0},{2,3},{3,2},{4,5},{5,4},{6,7},{7,6},{8,9},{9,8},{10,11... | collective-permute-start | bytes 3145736 | tf_op jit(solution)/shard_map/ppermute | solution.py:271
  20.8 14.6 %collective-permute-start.3 = (bf16[512,512]{1,0:T(8,128)(2,1)}, bf16[512,512]{1,0:T(8,128)(2,1)}, u32[]{:S(2)}, u32[]{:S(2)}) collective-permute-start(bf16[512,512]{1,0:T(8,128)(2,1)} %quarters.3), channel_id=1, source_target_pairs={{0,2},{1,3},{2,0},{3,1},{4,6},{5,7},{6,4},{7,5},{8,10},{9,11},{10,... | collective-permute-start | bytes 1572872 | tf_op jit(solution)/shard_map/ppermute | solution.py:282
  22.6 14.2 %collective-permute-start.2 = (bf16[512,512]{1,0:T(8,128)(2,1)}, bf16[512,512]{1,0:T(8,128)(2,1)}, u32[]{:S(2)}, u32[]{:S(2)}) collective-permute-start(bf16[512,512]{1,0:T(8,128)(2,1)} %collective-permute-done.refs_0_), channel_id=1, source_target_pairs={{0,8},{4,12},{8,0},{12,4},{16,24},{20,28},{24,16},{28,20},{1,9},{5... | collective-permute-start | bytes 1572872 | tf_op jit(solution)/shard_map/ppermute | solution.py:274
  24.2 13.9 %collective-permute-start.1 = (bf16[512,512]{1,0:T(8,128)(2,1)}, bf16[512,512]{1,0:T(8,128)(2,1)}, u32[]{:S(2)}, u32[]{:S(2)}) collective-permute-start(bf16[512,512]{1,0:T(8,128)(2,1)} %collective-permute-done.refs_0_), channel_id=1, source_target_pairs={{0,4},{4,0},{8,12},{12,8},{16,20},{20,16},{24,28},{28,24},{1,5},{5... | collective-permute-start | bytes 1572872 | tf_op jit(solution)/shard_map/ppermute | solution.py:274
  41.4 5.5 %collective-permute-start.8 = (bf16[256,512]{1,0:T(8,128)(2,1)}, bf16[256,512]{1,0:T(8,128)(2,1)}, u32[]{:S(2)}, u32[]{:S(2)}) collective-permute-start(bf16[256,512]{1,0:T(8,128)(2,1)} %project.7), channel_id=1, source_target_pairs={{0,1},{1,0},{2,3},{3,2},{4,5},{5,4},{6,7},{7,6},{8,9},{9,8},{10,11... | collective-permute-start | bytes 786440 | tf_op jit(solution)/shard_map/ppermute | solution.py:271
  44.1 2.8 %collective-permute-start.7 = (bf16[256,512]{1,0:T(8,128)(2,1)}, bf16[256,512]{1,0:T(8,128)(2,1)S(1)}, u32[]{:S(2)}, u32[]{:S(2)}) collective-permute-start(bf16[256,512]{1,0:T(8,128)(2,1)} %project.6), channel_id=1, source_target_pairs={{0,1},{1,0},{2,3},{3,2},{4,5},{5,4},{6,7},{7,6},{8,9},{9,8},{10,11... | collective-permute-start | bytes 786440 | tf_op jit(solution)/shard_map/ppermute | solution.py:271
